TPU v7x, 512 devices: a whole 4x8x8 slice. The times are simulated.
512 devices in a mesh: sp: 64 (over z, y), dp: 8 (over x, core).
Axes of the slice: x: 4, y: 8, z: 8, core: 2. Of those that a mesh axis runs over, the one named last changes fastest.
Arguments:
- inputs: bfloat16 [8, 8192, 2048], P('dp', 'sp'), may hold values from -6 to 6
- conv_weight: bfloat16 [4, 2048], replicated, may hold values from -3 to 3
- gate_weight: bfloat16 [2, 8, 256, 256], P(None, 'dp'), may hold values from -0.375 to 0.375
- rate_param: float32 [2048], replicated, may hold values from 4 to 12.5
- pace: float32 [8, 8192], P('dp'), may hold values from 0.5 to 30000
Outputs:
- recurrent: bfloat16 [8, 8192, 2048], P('dp', 'sp')
All inputs are finite; a program needn't handle non-finite values.
Results may differ from a plain program's by a relative error of at most 0.008.
Values may be sent and summed in bfloat16 or wider, within the bound.
No kernel may reach another device: no remote copies, remote signals or barrier semaphores. Data moves between devices by JAX's collectives and lax.ppermute only.
A program may use at most 128 MiB of HBM per device.

v0:
```python
import jax
import jax.numpy as jnp
from jax import lax
from jax.sharding import Mesh
from jax.sharding import PartitionSpec as P

HEADS = 8
BLOCK = 256
CONV = 4
DP = ("dp_0", "dp_1")


gate_power = 8.0


def passed_along(array, axis, by):
    devices = lax.axis_size(axis)
    pairs = [(i, i + by) for i in range(devices) if 0 <= i + by < devices]
    return lax.ppermute(array, axis, pairs)


def piece_ends(length, count):
    unit = 8 if length >= 8 * count else 1
    return [length // unit * k // count * unit for k in range(1, count)]


def gather_in_order(array, axes, sequence):
    pieces = array[None]
    for k in sequence:
        pieces = lax.all_gather(pieces, axes[k], axis=0, tiled=True)
    block = [lax.axis_size(axes[k]) for k in reversed(sequence)]
    pieces = pieces.reshape(*block, *array.shape)
    turned = sorted(range(len(sequence)), key=lambda place: sequence[len(sequence) - 1 - place])
    return pieces.transpose(*turned, *range(len(sequence), pieces.ndim)).reshape(-1, *array.shape)


def joined_along(pieces, dim):
    lengths = list(pieces.shape[1:])
    lengths[dim] *= pieces.shape[0]
    return jnp.moveaxis(pieces, 0, dim).reshape(lengths)


def gather_all_axes(array, axes, dim):
    widest = max(range(max(1, array.ndim - 1)), key=lambda d: array.shape[d])
    count, outs = (len(axes), [])
    for leading, section in enumerate(
        jnp.split(array, piece_ends(array.shape[widest], count), axis=widest)
    ):
        if section.size:
            sequence = [(leading - k) % count for k in range(count)]
            outs.append(gather_in_order(section, axes, sequence))
    return joined_along(jnp.concatenate(outs, axis=widest + 1), dim)


def from_everyone(array, axis):
    copies = jnp.broadcast_to(array, (lax.axis_size(axis), *array.shape))
    return lax.all_to_all(copies, axis, split_axis=0, concat_axis=0, tiled=True)


def gathered_once(array, axis):
    leaves = jax.tree.leaves(array)
    sequence = sorted(range(len(leaves)), key=lambda k: -leaves[k].size)
    width = (1, *leaves[sequence[0]].shape)[-1]
    lines = [
        jnp.pad(leaves[k].reshape(-1), (0, -leaves[k].size % width)).reshape(-1, width)
        for k in sequence
    ]
    both, at, found = (from_everyone(jnp.concatenate(lines), axis), 0, {})
    for k, line in zip(sequence, lines):
        section = both[:, at : at + len(line)].reshape(len(both), -1)
        found[k] = section[:, : leaves[k].size].reshape(-1, *leaves[k].shape)
        at += len(line)
    numbers = iter(range(len(leaves)))
    return jax.tree.map(lambda _: found[next(numbers)], array)


def combined_pairwise(pieces, combine):
    while len(jax.tree.leaves(pieces)[0]) > 1:
        pieces = jax.vmap(combine)(
            *(jax.tree.map(lambda part: part[side::2], pieces) for side in (0, 1))
        )
    return jax.tree.map(lambda part: part[0], pieces)


def prefix(array, axis, combine, identity):
    devices, here = (lax.axis_size(axis), lax.axis_index(axis))
    passed = jnp.arange(devices) < here

    def kept(part, zero, own):
        part = jnp.where(
            passed.reshape(-1, *(1 for _ in own.shape)), part, jnp.asarray(zero, own.dtype)
        )
        return part

    pieces = gathered_once(array, axis)
    return combined_pairwise(jax.tree.map(kept, pieces, identity, array), combine)


def combine(earlier, later):
    decay_e, state_e = earlier
    decay_l, state_l = later
    return (decay_e * decay_l, decay_l * state_e + state_l)


def lru_terms(pre_recur, pre_input, values, rate_col, pace_col):
    recur_gate = jax.nn.sigmoid(pre_recur.astype(jnp.float32))
    input_gate = jax.nn.sigmoid(pre_input.astype(jnp.float32))
    log_decay = -gate_power * pace_col * recur_gate * jax.nn.softplus(-rate_col)
    decay = jnp.exp(log_decay)
    drive = jnp.sqrt(-jnp.expm1(2.0 * log_decay)) * input_gate * values.astype(jnp.float32)
    return (decay, drive)


def body(inputs, conv_weight, gate_weight, rate_param, pace):
    own_rows = inputs[0].T
    width = own_rows.shape[0]
    count = own_rows.shape[1]
    earlier = passed_along(own_rows[:, count - (CONV - 1) :], "sp", 1)
    padded = jnp.concatenate([earlier, own_rows], axis=1).astype(jnp.float32)
    conv_taps = conv_weight.astype(jnp.float32)
    conv_out = jnp.zeros((width, count), jnp.float32)
    for tap in range(CONV):
        conv_out = conv_out + conv_taps[tap][:, None] * padded[:, tap : tap + count]
    conv_out = conv_out.astype(jnp.bfloat16)
    by_head = conv_out.reshape(HEADS, BLOCK, count)
    preact = (
        jnp.einsum(
            "hit,ghij->ghjt",
            by_head,
            gather_all_axes(gate_weight, DP, 1),
            preferred_element_type=jnp.float32,
        )
        .astype(jnp.bfloat16)
        .reshape(2, width, count)
    )
    own_pace = lax.dynamic_slice_in_dim(pace[0], lax.axis_index("sp") * count, count)
    decay, drive = lru_terms(preact[0], preact[1], conv_out, rate_param[:, None], own_pace[None, :])
    decay_run, state = lax.associative_scan(combine, (decay, drive), axis=1)
    identity = (jnp.ones((width,), jnp.float32), jnp.zeros((width,), jnp.float32))
    _, carried = prefix((decay_run[:, -1], state[:, -1]), "sp", combine, identity)
    result = (state + decay_run * carried[:, None]).astype(jnp.bfloat16)
    return result.T[None]


def solution(mesh):
    finer = Mesh(mesh.devices.reshape(mesh.shape["sp"], 4, 2), ("sp", "dp_0", "dp_1"))
    in_specs = (P(DP, "sp", None), P(), P(None, DP, None, None), P(), P(DP, None))
    out_specs = P(DP, "sp", None)
    return jax.shard_map(body, mesh=finer, in_specs=in_specs, out_specs=out_specs, check_vma=False)
```

profile of v0, /device:TPU:8, one launch (start us, length us, event | category | flops | bytes accessed | tf_op | source)
XLA Modules:
  0.0 180.7 jit_solution(7112969151282541759)
XLA Ops:
  6.5 1.0 fusion.24
  7.6 13.9 %all-gather = bf16[8,1,128,256]{3,2,1,0:T(8,128)(2,1)} all-gather(bf16[2,1,128,256]{3,2,1,0:T(8,128)(2,1)S(1)} %get-tuple-element.21), channel_id=2, replica_groups=mesh['sp'=64,'dp_0'=4,'dp_1'=2] {'dp_0'}, dimensions={0}, use_global_device_ids=true | all-gather | bytes 655360 | tf_op jit(solution)/shard_map/all_gather | solution.py:30
  21.5 2.1 %all-gather.1 = bf16[4,1,128,256]{3,2,1,0:T(8,128)(2,1)} all-gather(bf16[2,1,128,256]{3,2,1,0:T(8,128)(2,1)S(1)} %get-tuple-element.22), channel_id=3, replica_groups=mesh['sp'=64,'dp_0'=4,'dp_1'=2] {'dp_1'}, dimensions={0}, use_global_device_ids=true | all-gather | bytes 393216 | tf_op jit(solution)/shard_map/all_gather | solution.py:30
  23.7 3.5 %collective-permute-start = (bf16[2048,3]{0,1:T(4,128)(2,1)S(1)}, bf16[2048,3]{0,1:T(4,128)(2,1)S(1)}, u32[]{:S(2)}, u32[]{:S(2)}) collective-permute-start(bf16[2048,3]{0,1:T(4,128)(2,1)S(1)} %slice.422), channel_id=1, source_target_pairs={{0,8},{8,16},{16,24},{24,32},{32,40},{40,48},{48,56},{56,64},{64,7... | collective-permute-start | bytes 36872 | tf_op jit(solution)/shard_map/ppermute | solution.py:19
  27.3 0.7 multiply_bitcast_fusion
  28.0 4.3 %collective-permute-done = bf16[2048,3]{0,1:T(4,128)(2,1)S(1)} collective-permute-done((bf16[2048,3]{0,1:T(4,128)(2,1)S(1)}, bf16[2048,3]{0,1:T(4,128)(2,1)S(1)}, u32[]{:S(2)}, u32[]{:S(2)}) %collective-permute-start) | collective-permute-done | bytes 12320 | tf_op jit(solution)/shard_map/ppermute | solution.py:19
  32.4 0.5 fusion.6
  32.9 1.0 copy.24
  33.9 9.5 %all-gather.5.cloned.1.call-done = bf16[8,2,1,128,256]{4,3,2,1,0:T(8,128)(2,1)} async-done(((bf16[4,2,1,128,256]{4,3,2,1,0:T(8,128)(2,1)}), bf16[8,2,1,128,256]{4,3,2,1,0:T(8,128)(2,1)}) %all-gather.5.cloned.1.call-update) | async-done | bytes 1048592 | tf_op jit(solution)/shard_map/all_gather | solution.py:30
  43.4 1.6 copy.16
  45.1 31.2 %all-gather.7.cloned.1.call-done = bf16[8,2,1,128,256]{4,3,2,1,0:T(8,128)(2,1)} async-done(((bf16[2,2,1,128,256]{4,3,2,1,0:T(8,128)(2,1)}), bf16[8,2,1,128,256]{4,3,2,1,0:T(8,128)(2,1)}) %all-gather.7.cloned.1.call-update) | async-done | bytes 1048592 | tf_op jit(solution)/shard_map/all_gather | solution.py:30
  76.3 1.6 copy.18
  77.9 1.7 fusion.4
  79.7 0.6 add_divide_fusion
  80.2 1.3 copy.21
  81.6 1.3 copy.20
  82.9 2.8 %convert_multiply_fusion = (f32[2048,128]{0,1:T(8,128)S(1)}, f32[2048,128]{0,1:T(8,128)S(1)}) fusion(f32[2048,128]{0,1:T(8,128)} %copy.21, f32[2048,128]{0,1:T(8,128)} %copy.20, f32[2048]{0:T(1024)S(1)} %compare_select_fusion, f32[128]{0:T(128)S(1)} %multiply_bitcast_fusion, f32[2048,131]{0,1:T(8,128)S(1)} %maximum_convert_fusion, f32[2048]{0:T(1024)S(1)} %bitcast.69, ...), kind=kLoop, calls=%fused_computation.15 | loop fusion | flops 3932160 | bytes 8430080 | tf_op jit(solution)/shard_map/mul | solution.py:110
  85.7 1.5 slice.380
  87.2 1.5 slice.334
  88.7 1.5 slice.333
  90.2 1.5 slice.336
  91.6 1.5 slice.332
  93.1 1.5 slice.331
  94.6 1.3 multiply_add_fusion
  96.0 0.2 slice.378
  99.8 0.9 add.221
  100.7 0.9 add.213
  101.6 0.4 copy-done.2
  102.1 0.2 fusion.11
  102.7 2.1 %pad.99 = f32[2048,128]{0,1:T(8,128)S(1)} pad(f32[2048,64]{0,1:T(8,128)} %add.213, f32[]{:T(128)} %constant.8.clone.1), padding=0_0_0x1_0_1 | pad | bytes 1572868 | tf_op jit(solution)/shard_map/pad | solution.py:138
  104.8 4.6 %pad.113 = f32[2048,128]{0,1:T(8,128)} pad(f32[2048,64]{0,1:T(8,128)} %add.221, f32[]{:T(128)} %constant.8.clone.1), padding=0_0_0x1_0_1 | pad | bytes 1572868 | tf_op jit(solution)/shard_map/pad | solution.py:138
  109.5 0.9 add_bitcast_fusion.1
  110.4 1.5 broadcast_in_dim.37
  111.9 13.6 %all-to-all-start = ((f32[64,2,2048]{2,1,0:T(2,128)}), f32[64,2,2048]{2,1,0:T(2,128)}, u32[]{:S(2)}, u32[]{:S(2)}) async-start(f32[64,2,2048]{2,1,0:T(2,128)} %broadcast_in_dim.37), calls=%async_computation | async-start | bytes 2097152 | tf_op jit(solution)/shard_map/all_to_all | solution.py:57
  125.5 27.8 %all-to-all-done = f32[64,2,2048]{2,1,0:T(2,128)} async-done(((f32[64,2,2048]{2,1,0:T(2,128)}), f32[64,2,2048]{2,1,0:T(2,128)}, u32[]{:S(2)}, u32[]{:S(2)}) %all-to-all-start) | async-done | bytes 1048608 | tf_op jit(solution)/shard_map/all_to_all | solution.py:57
  153.2 2.6 %fusion.22 = (f32[64,1,2048]{2,1,0:T(1,128)S(1)}, f32[64,1,2048]{2,1,0:T(1,128)S(1)}) fusion(f32[64,2,2048]{2,1,0:T(2,128)} %all-to-all-done), kind=kLoop, calls=%fused_computation.86 | loop fusion | bytes 2097152 | tf_op jit(solution)/shard_map/slice | solution.py:70
  155.8 1.4 fusion.12
  157.2 1.7 slice.398
  158.9 1.7 slice.397
  160.6 1.7 slice.410
  162.3 1.7 slice.409
  164.0 1.9 %fusion.23 = (f32[32,2048]{1,0:T(8,128)}, f32[32,2048]{1,0:T(8,128)S(1)}) fusion(f32[32,2048]{1,0:T(8,128)} %slice.397, f32[32,2048]{1,0:T(8,128)} %slice.398, f32[32,2048]{1,0:T(8,128)} %slice.410, f32[32,2048]{1,0:T(8,128)} %slice.409), kind=kLoop, calls=%fused_computation.87 | loop fusion | flops 196608 | bytes 1572864 | tf_op jit(solution)/shard_map/vmap()/mul | solution.py:102
  166.0 1.0 slice.400
  166.9 1.6 slice.399
  168.6 0.7 slice.412
  169.3 0.7 slice.411
  169.9 1.1 fusion.25
  171.5 2.3 %fusion.10 = bf16[1,128,2048]{2,1,0:T(8,128)(2,1)} fusion(f32[2048,128]{0,1:T(8,128)S(1)} %pad.112, f32[2048,128]{0,1:T(8,128)} %pad.113, f32[2048,128]{0,1:T(8,128)S(1)} %pad.98, f32[2048,128]{0,1:T(8,128)S(1)} %pad.99, f32[2048]{0:T(1024)S(1)} %bitcast.70), kind=kLoop, calls=%fused_computation.21 | loop fusion | flops 1310720 | bytes 4726784 | tf_op jit(solution)/shard_map/broadcast_in_dim | solution.py:142
  (130 shorter events, 4.5 us)
Async XLA Ops:
  6.5 17.2 %copy-start.4 = (bf16[1,128,2048]{2,1,0:T(8,128)(2,1)S(1)}, bf16[1,128,2048]{2,1,0:T(8,128)(2,1)}, u32[]{:S(2)}) copy-start(bf16[1,128,2048]{2,1,0:T(8,128)(2,1)} %param.5) | copy-start | bytes 1572868
  6.5 20.7 %copy-start.6 = (f32[2048]{0:T(1024)S(1)}, f32[2048]{0:T(1024)}, u32[]{:S(2)}) copy-start(f32[2048]{0:T(1024)} %param.8) | copy-start | bytes 24580
  6.5 20.7 %copy-start.5 = (bf16[4,2048]{1,0:T(4,128)(2,1)S(1)}, bf16[4,2048]{1,0:T(4,128)(2,1)}, u32[]{:S(2)}) copy-start(bf16[4,2048]{1,0:T(4,128)(2,1)} %param.6) | copy-start | bytes 49156
  6.5 36.9 %all-gather.5.cloned.1.call-start = ((), (), s32[]{:S(2)}) async-start(), calls=%async_computation.1 | async-start | bytes 1572864 | tf_op jit(solution)/shard_map/all_gather | solution.py:30
  21.5 54.8 %all-gather.7.cloned.1.call-start = ((), (), s32[]{:S(2)}) async-start(), calls=%async_computation.2 | async-start | bytes 1310720 | tf_op jit(solution)/shard_map/all_gather | solution.py:30
  23.7 8.6 %collective-permute-start = (bf16[2048,3]{0,1:T(4,128)(2,1)S(1)}, bf16[2048,3]{0,1:T(4,128)(2,1)S(1)}, u32[]{:S(2)}, u32[]{:S(2)}) collective-permute-start(bf16[2048,3]{0,1:T(4,128)(2,1)S(1)} %slice.422), channel_id=1, source_target_pairs={{0,8},{8,16},{16,24},{24,32},{32,40},{40,48},{48,56},{56,64},{64,7... | collective-permute-start | bytes 36872 | tf_op jit(solution)/shard_map/ppermute | solution.py:19
  91.6 3.0 %copy-start = (f32[2048,64]{0,1:T(8,128)S(1)}, f32[2048,64]{0,1:T(8,128)}, u32[]{:S(2)}) copy-start(f32[2048,64]{0,1:T(8,128)} %slice.334) | copy-start | bytes 1572868
  91.6 3.0 %copy-start.1 = (f32[2048,64]{0,1:T(8,128)S(1)}, f32[2048,64]{0,1:T(8,128)}, u32[]{:S(2)}) copy-start(f32[2048,64]{0,1:T(8,128)} %slice.333) | copy-start | bytes 1572868
  100.7 1.2 copy-start.2
  100.7 1.4 copy-start.3
  111.9 41.4 %all-to-all-start = ((f32[64,2,2048]{2,1,0:T(2,128)}), f32[64,2,2048]{2,1,0:T(2,128)}, u32[]{:S(2)}, u32[]{:S(2)}) async-start(f32[64,2,2048]{2,1,0:T(2,128)} %broadcast_in_dim.37), calls=%async_computation | async-start | bytes 2097152 | tf_op jit(solution)/shard_map/all_to_all | solution.py:57
Sparse Core Ops, SparseCore 0:
  21.6 21.7 all-gather.4
  45.5 30.7 all-gather.6
where the time goes:
time: 182 us; the launch traced here: 181 us
  waiting for transfers between devices  72.9 us (40%)
  local copies, waits for them, and re-layouts  42.2 us (23%)
  starting transfers between devices  17.1 us (9%)
  other arithmetic  16.5 us (9%)
  blocking collectives  16 us (9%)
  between operations  14.2 us (8%)
    all_gather x2, waiting for transfers between devices, gather_in_order(): pieces = lax.all_gather(pieces, axes[k], axis=0, tiled=True)  40.8 us
    all_to_all x1, waiting for transfers between devices, from_everyone(): return lax.all_to_all(copies, axis, split_axis=0, concat_axis=0, tiled=True)  27.8 us
    all_gather x2, blocking collectives, gather_in_order(): pieces = lax.all_gather(pieces, axes[k], axis=0, tiled=True)  16 us
    all_to_all x1, starting transfers between devices, from_everyone(): return lax.all_to_all(copies, axis, split_axis=0, concat_axis=0, tiled=True)  13.6 us
    slice x20, local copies, waits for them, and re-layouts, combined_pairwise(): part[side::2]  11.1 us
    slice x44, local copies, waits for them, and re-layouts, body(): decay_run, state = lax.associative_scan(combine, (decay, drive), axis=1)  10.8 us
    pad x24, local copies, waits for them, and re-layouts, body(): decay_run, state = lax.associative_scan(combine, (decay, drive), axis=1)  7.74 us
    ppermute x1, waiting for transfers between devices, passed_along(): return lax.ppermute(array, axis, pairs)  4.33 us
  transfers between devices with their start and end apart: 4, of which 4 were waited for; matrix products, arithmetic and copies ran while one was open for 2% of the time, Pallas kernels for 0%

commit v1 on v0

v1 whole, which is shorter than its diff:
```python
import functools

import jax
import jax.numpy as jnp
from jax import lax
from jax.experimental import pallas as pl
from jax.experimental.pallas import tpu as pltpu
from jax.sharding import Mesh
from jax.sharding import PartitionSpec as P

HEADS = 8
BLOCK = 256
CONV = 4
ROWS = 128
CHUNKS = 8
STEPS = ROWS // CHUNKS
LANES = 128

gate_power = 8.0
f32, bf16 = jnp.float32, jnp.bfloat16


def order_matrix(transposed):
    here = lax.broadcasted_iota(jnp.int32, (ROWS, ROWS), 1 if transposed else 0)
    position = lax.broadcasted_iota(jnp.int32, (ROWS, ROWS), 0 if transposed else 1)
    return position == (here & (CHUNKS - 1)) * STEPS + (here >> 3)


def softplus_of_minus(rate):
    e = jnp.exp(-jnp.abs(rate))
    series = e * (1 - e * (1 / 2 - e * (1 / 3 - e * (1 / 4 - e * (1 / 5 - e * (1 / 6))))))
    return jnp.maximum(-rate, 0.0) + jnp.where(e < 0.05, series, jnp.log(1.0 + e))


def sublane_before(tile, shift, fill):
    row = lax.broadcasted_iota(jnp.int32, tile.shape, 0)
    return jnp.where(row < shift, fill, pltpu.roll(tile, shift, 0))


def conv_all(x_ref, halo_ref, cw_ref, cv_ref):
    perm = order_matrix(False).astype(bf16)
    for h in range(HEADS):
        cols = pl.ds(h * BLOCK, BLOCK)
        moved = jnp.dot(perm, x_ref[:, cols], preferred_element_type=f32)
        step = [moved[CHUNKS * r : CHUNKS * (r + 1)] for r in range(STEPS)]
        halo = halo_ref[:, cols].astype(f32)
        taps = cw_ref[:, cols].astype(f32)
        early = [
            sublane_before(step[STEPS - j], 1, halo[8 - j : 9 - j]) for j in (3, 2, 1)
        ]
        line = early + step
        for r in range(0, STEPS, 2):
            both = []
            for q in (r, r + 1):
                total = taps[0:1] * line[q]
                for tap in range(1, CONV):
                    total = total + taps[tap : tap + 1] * line[q + tap]
                both.append(total)
            cv_ref[pl.ds(CHUNKS * r, 2 * CHUNKS), cols] = jnp.concatenate(both, 0).astype(bf16)


def one_head(head, cv_ref, w0, w1, pace_ref, rate_ref, pre_ref, h_ref, p_ref, edge_ref, slot):
    cols = pl.ds(pl.multiple_of(head * BLOCK, BLOCK), BLOCK)
    values = cv_ref[:, cols]
    pre_ref[0] = jnp.dot(values, w0, preferred_element_type=f32)
    pre_ref[1] = jnp.dot(values, w1, preferred_element_type=f32)
    pre_ref[2] = values.astype(f32)
    soft = gate_power * softplus_of_minus(rate_ref[:, cols])
    totals = []
    for lane in range(0, BLOCK, LANES):
        at = slice(lane, lane + LANES)
        soft_here = soft[:, at]
        state = run = used = None
        for r in range(STEPS):
            rows = slice(CHUNKS * r, CHUNKS * (r + 1))
            x0 = pre_ref[0, rows, at].astype(bf16).astype(f32)
            x1 = pre_ref[1, rows, at].astype(bf16).astype(f32)
            recur_gate = 1.0 / (1.0 + jnp.exp(-x0))
            input_gate = 1.0 / (1.0 + jnp.exp(-x1))
            loss = pace_ref[rows, :] * recur_gate * soft_here
            decay = jnp.exp(-loss)
            v = 2.0 * loss
            series = v * (1 - v * (1 / 2 - v * (1 / 6 - v * (1 / 24 - v * (1 / 120)))))
            gone = jnp.where(v < 0.1, series, 1.0 - decay * decay)
            drive = jnp.sqrt(gone) * input_gate * pre_ref[2, rows, at]
            if r == 0:
                state, run, used = drive, decay, loss
            else:
                state, run, used = decay * state + drive, decay * run, used + loss
            h_ref[slot, rows, at] = state
            p_ref[slot, rows, at] = run
        for shift in (1, 2, 4):
            state = state + run * sublane_before(state, shift, 0.0)
            run = run * sublane_before(run, shift, 1.0)
        edge_ref[slot, 0, :, at] = sublane_before(state, 1, 0.0)
        edge_ref[slot, 1, :, at] = sublane_before(run, 1, 1.0)
        totals.append((jnp.sum(used, 0, keepdims=True), state[CHUNKS - 1 : CHUNKS]))
    return tuple(jnp.concatenate([t[k] for t in totals], 1) for k in (0, 1))


def chips():
    x, c = lax.axis_index("dp_0"), lax.axis_index("dp_1")
    near = jnp.where(c == 0, x + 3, x + 1) & 3
    other = jnp.where(c == 0, x + 1, x + 3) & 3
    return x, c, near, other, (x + 2) & 3


def heads_of(group):
    x, c, near, other, far = chips()
    return {
        "own": [2 * x, 2 * x + 1],
        "near": [2 * near, 2 * near + 1, 2 * far + c],
        "rest": [2 * other, 2 * other + 1, 2 * far + 1 - c],
    }[group]


def own_kernel(x_ref, halo_ref, cw_ref, rate_ref, pace_ref, w_ref, cv_ref, pcol_ref, h_ref, p_ref, edge_ref, tot_ref, pre_ref):
    here = lax.axis_index("sp")
    pace = pace_ref[:, pl.ds(pl.multiple_of(here * ROWS, ROWS), ROWS)]
    column = jnp.sum(jnp.where(order_matrix(False), pace, 0.0), axis=1, keepdims=True)
    pcol_ref[...] = jnp.broadcast_to(column, (ROWS, LANES))
    conv_all(x_ref, halo_ref, cw_ref, cv_ref)
    for slot, head in enumerate(heads_of("own")):
        used, state = one_head(head, cv_ref, w_ref[slot, 0], w_ref[slot, 1], pcol_ref, rate_ref, pre_ref, h_ref, p_ref, edge_ref, slot)
        tot_ref[0, slot : slot + 1] = used
        tot_ref[1, slot : slot + 1] = state


def near_kernel(cv_ref, pcol_ref, rate_ref, wa_ref, wb_ref, h_ref, p_ref, edge_ref, tot_ref, pre_ref):
    for slot, head in enumerate(heads_of("near")):
        w = wb_ref if slot == 2 else wa_ref.at[slot]
        used, state = one_head(head, cv_ref, w[0], w[1], pcol_ref, rate_ref, pre_ref, h_ref, p_ref, edge_ref, slot)
        tot_ref[0, slot : slot + 1] = used
        tot_ref[1, slot : slot + 1] = state


def rest_kernel(cv_ref, pcol_ref, rate_ref, wa_ref, wb_ref, own_ref, near_ref, h_ref, p_ref, edge_ref, send_ref, pre_ref):
    totals = []
    for slot, head in enumerate(heads_of("rest")):
        w = wb_ref if slot == 2 else wa_ref.at[slot]
        totals.append(one_head(head, cv_ref, w[0], w[1], pcol_ref, rate_ref, pre_ref, h_ref, p_ref, edge_ref, slot))
    lines = []
    for k in (0, 1):
        lines += [own_ref[k, 0:2], near_ref[k, 0:3]] + [t[k] for t in totals]
    message = jnp.concatenate(lines, 0).astype(bf16)

    def put(j, _):
        send_ref[j] = message
        return 0

    lax.fori_loop(0, send_ref.shape[0], put, 0, unroll=8)


def last_kernel(all_ref, *refs):
    groups, out_ref = refs[:9], refs[9]
    here = lax.axis_index("sp")
    count = all_ref.shape[0]
    parts = []
    for first in range(0, count, 8):
        state = run = None
        for j in range(first, first + 8):
            line = all_ref[j].astype(f32)
            mine = (j < here).astype(f32)
            decay = jnp.exp(-(line[:HEADS] * mine))
            drive = line[HEADS:] * mine
            if state is None:
                state, run = drive, decay
            else:
                state, run = decay * state + drive, decay * run
        parts.append((run, state))
    carried = parts[0][1]
    for run, state in parts[1:]:
        carried = run * carried + state
    back = order_matrix(True).astype(bf16)
    at = 0
    for g, name in enumerate(("own", "near", "rest")):
        h_ref, p_ref, edge_ref = groups[3 * g : 3 * g + 3]
        for slot, head in enumerate(heads_of(name)):
            enters = edge_ref[slot, 0] + edge_ref[slot, 1] * carried[at : at + 1]
            whole = h_ref[slot].reshape(STEPS, CHUNKS, BLOCK) + p_ref[slot].reshape(
                STEPS, CHUNKS, BLOCK
            ) * enters.reshape(1, CHUNKS, BLOCK)
            rounded = whole.reshape(ROWS, BLOCK).astype(bf16)
            cols = pl.ds(pl.multiple_of(head * BLOCK, BLOCK), BLOCK)
            out_ref[:, cols] = jnp.dot(back, rounded, preferred_element_type=f32).astype(bf16)
            at += 1


def vmem(count):
    return [pl.BlockSpec(memory_space=pltpu.VMEM)] * count


def call(kernel, outs, args, name, scratch=True, us=2.0):
    return pl.pallas_call(
        kernel,
        name=name,
        out_shape=[jax.ShapeDtypeStruct(s, d) for s, d in outs],
        in_specs=vmem(len(args)),
        out_specs=vmem(len(outs)),
        scratch_shapes=[pltpu.VMEM((3, ROWS, BLOCK), f32)] if scratch else [],
        compiler_params=pltpu.CompilerParams(vmem_limit_bytes=16 * 2**20),
        cost_estimate=pl.CostEstimate(flops=int(us * 2e8), bytes_accessed=1 << 20, transcendentals=1 << 18),
    )(*args)


def head_outs(n):
    return [((n, ROWS, BLOCK), f32), ((n, ROWS, BLOCK), f32), ((n, 2, CHUNKS, BLOCK), f32)]


def body(inputs, conv_weight, gate_weight, rate_param, pace):
    x = inputs[0]
    rate = rate_param[None]
    devices = lax.axis_size("sp")
    dp = ("dp_0", "dp_1")
    core = [(0, 1), (1, 0)]
    own = gate_weight[:, 0]
    pair = lax.all_gather(own, "dp_1")
    near = lax.ppermute(
        pair, dp, [(2 * i + k, 2 * ((i + (1, 3)[k]) % 4) + k) for i in range(4) for k in (0, 1)]
    )
    far = lax.ppermute(own, "dp_0", [(i, (i + 2) % 4) for i in range(4)])
    halo = lax.ppermute(x[ROWS - 8 :], "sp", [(i, i + 1) for i in range(devices - 1)])
    cv, pcol, *own_out, own_tot = call(
        own_kernel,
        [((ROWS, HEADS * BLOCK), bf16), ((ROWS, LANES), f32), *head_outs(2), ((2, 2, BLOCK), f32)],
        (x, halo, conv_weight, rate, pace, pair),
        "own_heads",
    )
    other = lax.ppermute(near, "dp_1", core)
    other_far = lax.ppermute(far, "dp_1", core)
    *near_out, near_tot = call(
        near_kernel,
        [*head_outs(3), ((2, 3, BLOCK), f32)],
        (cv, pcol, rate, near, far),
        "near_heads",
    )
    *rest_out, send = call(
        rest_kernel,
        [*head_outs(3), ((devices, 2 * HEADS, BLOCK), bf16)],
        (cv, pcol, rate, other, other_far, own_tot, near_tot),
        "rest_heads",
    )
    everyone = lax.all_to_all(send, "sp", split_axis=0, concat_axis=0, tiled=True)
    (result,) = call(
        last_kernel,
        [((ROWS, HEADS * BLOCK), bf16)],
        (everyone, *own_out, *near_out, *rest_out),
        "carry_in",
        scratch=False,
    )
    return result[None]


def solution(mesh):
    finer = Mesh(mesh.devices.reshape(mesh.shape["sp"], 4, 2), ("sp", "dp_0", "dp_1"))
    dp = ("dp_0", "dp_1")
    in_specs = (P(dp, "sp", None), P(), P(None, dp, None, None), P(), P(dp, None))
    out_specs = P(dp, "sp", None)
    return jax.shard_map(body, mesh=finer, in_specs=in_specs, out_specs=out_specs, check_vma=False)
```

time: 182 us -> 72.2 us (0.40)
  waiting for transfers between devices: 72.9 us -> 13 us
  local copies, waits for them, and re-layouts: 42.2 us -> 0.03 us
  blocking collectives: 16 us -> 38.6 us
  other arithmetic: 16.5 us -> 0 us
  between operations: 14.2 us -> 0.13 us
  Pallas kernels: 0 us -> 4.16 us
    all_gather x2 -> x0, waiting for transfers between devices: 40.8 us -> none  [gather_in_order(): pieces = lax.all_gather(pieces, axes[k], axis=0, tiled=True)]
    all_to_all x0 -> x1, blocking collectives: none -> 36.1 us  [body(): lax.all_to_all(send, 'sp', split_axis=0, concat_axis=0, tiled=True)]
    all_to_all x1 -> x0, waiting for transfers between devices: 27.8 us -> none  [from_everyone(): return lax.all_to_all(copies, axis, split_axis=0, concat_axis=0, tiled=True)]
    slice x67 -> x1, local copies, waits for them, and re-layouts: 24.5 us -> 0.01 us  [body(): x[ROWS - 8:]]
    all_to_all x1 -> x0, starting transfers between devices: 13.6 us -> none  [from_everyone(): return lax.all_to_all(copies, axis, split_axis=0, concat_axis=0, tiled=True)]
    all_gather x2 -> x1, blocking collectives: 16 us -> 2.51 us  [body(): pair = lax.all_gather(own, 'dp_1')]
    ppermute x1 -> x5, starting transfers between devices: 3.48 us -> 16 us  [the longest x1 4.77 us: body(): far = lax.ppermute(own, 'dp_0', [(i, (i + 2) % 4) for i in range(4)])]
    ppermute x1 -> x5, waiting for transfers between devices: 4.33 us -> 13 us  [the longest x1 10.7 us: body(): far = lax.ppermute(own, 'dp_0', [(i, (i + 2) % 4) for i in range(4)])]
  transfers between devices with their start and end apart: 4 -> 5, of which waited for: 4 -> 2; matrix products, arithmetic and copies ran while one was open for 2% -> 0% of each run, Pallas kernels for 0% -> 3%
where the time goes in v1:
time: 72.2 us; the launch traced here: 71.9 us
  blocking collectives  38.6 us (53%)
  starting transfers between devices  16 us (22%)
  waiting for transfers between devices  13 us (18%)
  Pallas kernels  4.16 us (6%)
    all_to_all x1, blocking collectives, body(): lax.all_to_all(send, 'sp', split_axis=0, concat_axis=0, tiled=True)  36.1 us
    ppermute x1, waiting for transfers between devices, body(): far = lax.ppermute(own, 'dp_0', [(i, (i + 2) % 4) for i in range(4)])  10.7 us
    ppermute x1, starting transfers between devices, body(): far = lax.ppermute(own, 'dp_0', [(i, (i + 2) % 4) for i in range(4)])  4.77 us
    pallas_call x4, Pallas kernels, call(): pl.pallas_call(kernel, name=name, out_shape=[jax.ShapeDtypeStruct(s, d) f...  4.16 us
    ppermute x1, starting transfers between devices, body(): lax.ppermute(x[ROWS - 8:], 'sp', [(i, i + 1) for i in range(devices - 1)])  3.48 us
    ppermute x1, starting transfers between devices, body(): lax.ppermute(pair, dp, [(2 * i + k, 2 * ((i + (1, 3)[k]) % 4) + k) for i...  3.39 us
    all_gather x1, blocking collectives, body(): pair = lax.all_gather(own, 'dp_1')  2.51 us
    ppermute x1, starting transfers between devices, body(): other = lax.ppermute(near, 'dp_1', core)  2.41 us
  transfers between devices with their start and end apart: 5, of which 2 were waited for; matrix products, arithmetic and copies ran while one was open for 0% of the time, Pallas kernels for 3%

profile of v1, /device:TPU:8, one launch (start us, length us, event | category | flops | bytes accessed | tf_op | source)
XLA Modules:
  0.0 71.9 jit_solution(928763339770375232)
XLA Ops:
  0.0 0.0 copy-start.4
  0.0 0.0 copy-start
  0.0 2.5 %all-gather = bf16[4,1,256,256]{3,2,1,0:T(8,128)(2,1)S(1)} all-gather(bf16[2,1,256,256]{3,2,1,0:T(8,128)(2,1)} %param.7), channel_id=2, replica_groups=mesh['sp'=64,'dp_0'=4,'dp_1'=2] {'dp_1'}, dimensions={0}, use_global_device_ids=true | all-gather | bytes 786432 | tf_op jit(solution)/shard_map/all_gather | solution.py:217
  2.5 3.4 %collective-permute-start.1 = (bf16[2,2,256,256]{3,2,1,0:T(8,128)(2,1)S(1)}, bf16[2,2,256,256]{3,2,1,0:T(8,128)(2,1)S(1)}, u32[]{:S(2)}, u32[]{:S(2)}) collective-permute-start(bf16[2,2,256,256]{3,2,1,0:T(8,128)(2,1)S(1)} %bitcast.7), channel_id=1, source_target_pairs={{0,2},{1,7},{2,4},{3,1},{4,6},{5,3},{6,0},{7,5},{8,10},{9,15},{10,... | collective-permute-start | bytes 1572872 | tf_op jit(solution)/shard_map/ppermute | solution.py:218
  5.9 0.0 copy-done.4
  5.9 0.0 copy-start.1
  5.9 0.0 copy-start.2
  5.9 0.0 copy-start.3
  6.0 4.8 %collective-permute-start.3 = (bf16[2,256,256]{2,1,0:T(8,128)(2,1)S(1)}, bf16[2,256,256]{2,1,0:T(8,128)(2,1)S(1)}, u32[]{:S(2)}, u32[]{:S(2)}) collective-permute-start(bf16[2,256,256]{2,1,0:T(8,128)(2,1)S(1)} %bitcast.13), channel_id=1, source_target_pairs={{0,4},{2,6},{4,0},{6,2},{1,5},{3,7},{5,1},{7,3},{8,12},{10,14},{12... | collective-permute-start | bytes 786440 | tf_op jit(solution)/shard_map/ppermute | solution.py:221
  10.7 10.7 %collective-permute-done.3.wb_ref = bf16[2,256,256]{2,1,0:T(8,128)(2,1)S(1)} collective-permute-done((bf16[2,256,256]{2,1,0:T(8,128)(2,1)S(1)}, bf16[2,256,256]{2,1,0:T(8,128)(2,1)S(1)}, u32[]{:S(2)}, u32[]{:S(2)}) %collective-permute-start.3) | collective-permute-done | bytes 262176 | tf_op jit(solution)/shard_map/ppermute | solution.py:221
  21.4 1.9 %collective-permute-start.4 = (bf16[2,256,256]{2,1,0:T(8,128)(2,1)S(1)}, bf16[2,256,256]{2,1,0:T(8,128)(2,1)S(1)}, u32[]{:S(2)}, u32[]{:S(2)}) collective-permute-start(bf16[2,256,256]{2,1,0:T(8,128)(2,1)S(1)} %collective-permute-done.3.wb_ref), channel_id=1, source_target_pairs={{0,1},{1,0},{2,3},{3,2},{4,5},{5,4},{6,7},{7,6},{8,9},{9,8},{10,11... | collective-permute-start | bytes 786440 | tf_op jit(solution)/shard_map/ppermute | solution.py:230
  23.3 0.0 collective-permute-done.1.wa_ref
  23.3 2.4 %collective-permute-start.2 = (bf16[2,2,256,256]{3,2,1,0:T(8,128)(2,1)S(1)}, bf16[2,2,256,256]{3,2,1,0:T(8,128)(2,1)S(1)}, u32[]{:S(2)}, u32[]{:S(2)}) collective-permute-start(bf16[2,2,256,256]{3,2,1,0:T(8,128)(2,1)S(1)} %collective-permute-done.1.wa_ref), channel_id=1, source_target_pairs={{0,1},{1,0},{2,3},{3,2},{4,5},{5,4},{6,7},{7,6},{8,9},{9,8},{10,11... | collective-permute-start | bytes 1572872 | tf_op jit(solution)/shard_map/ppermute | solution.py:229
  25.7 0.0 copy-done
  25.8 3.5 %collective-permute-start = (bf16[8,2048]{1,0:T(8,128)(2,1)S(1)}, bf16[8,2048]{1,0:T(8,128)(2,1)S(1)}, u32[]{:S(2)}, u32[]{:S(2)}) collective-permute-start(bf16[8,2048]{1,0:T(8,128)(2,1)S(1)} %slice_bitcast_fusion), channel_id=1, source_target_pairs={{0,8},{8,16},{16,24},{24,32},{32,40},{40,48},{48,56},{56,64},{64,7... | collective-permute-start | bytes 98312 | tf_op jit(solution)/shard_map/ppermute | solution.py:222
  29.3 2.3 %collective-permute-done.halo_ref = bf16[8,2048]{1,0:T(8,128)(2,1)S(1)} collective-permute-done((bf16[8,2048]{1,0:T(8,128)(2,1)S(1)}, bf16[8,2048]{1,0:T(8,128)(2,1)S(1)}, u32[]{:S(2)}, u32[]{:S(2)}) %collective-permute-start) | collective-permute-done | bytes 32800 | tf_op jit(solution)/shard_map/ppermute | solution.py:222
  31.6 0.0 copy-done.1
  31.6 0.0 copy-done.2
  31.6 0.0 copy-done.3
  31.6 1.1 %own_heads.1 = (bf16[128,2048]{1,0:T(8,128)(2,1)S(1)}, f32[128,128]{1,0:T(8,128)S(1)}, f32[2,128,256]{2,1,0:T(8,128)S(1)}, f32[2,128,256]{2,1,0:T(8,128)S(1)}, f...) custom-call(bf16[128,2048]{1,0:T(8,128)(2,1)S(1)} %bitcast.9, bf16[8,2048]{1,0:T(8,128)(2,1)S(1)} %collective-permute-done.halo_ref, ...), custom_call_target="tpu_custom_call" | custom-call | flops 400000000 | bytes 1048576 | tf_op jit(solution)/shard_map/own_heads/pallas_call | solution.py:194
  32.6 0.9 %near_heads.1 = (f32[3,128,256]{2,1,0:T(8,128)S(1)}, f32[3,128,256]{2,1,0:T(8,128)S(1)}, f32[3,2,8,256]{3,2,1,0:T(8,128)S(1)}, f32[2,3,256]{2,1,0:T(4,128)S(1)}) custom-call(bf16[128,2048]{1,0:T(8,128)(2,1)S(1)} %get-tuple-element.19.cv_ref, f32[128,128]{1,0:T(8,128)S(1)} %get-tuple-element.20.pcol_ref, f32[1,2048]{1,0:T(1,128)S(1)} %bitcast.11, ...), custom_call_target="tpu_custom_call" | custom-call | flops 400000000 | bytes 1048576 | tf_op jit(solution)/shard_map/near_heads/pallas_call | solution.py:194
  33.5 0.0 collective-permute-done.4.wb_ref
  33.5 0.0 collective-permute-done.2.wa_ref
  33.5 0.9 %rest_heads.1 = (f32[3,128,256]{2,1,0:T(8,128)S(1)}, f32[3,128,256]{2,1,0:T(8,128)S(1)}, f32[3,2,8,256]{3,2,1,0:T(8,128)S(1)}, bf16[64,16,256]{2,1,0:T(8,128)(2,1)S(1)}) custom-call(bf16[128,2048]{1,0:T(8,128)(2,1)S(1)} %get-tuple-element.19.cv_ref, f32[128,128]{1,0:T(8,128)S(1)} %get-tuple-element.20.pcol_ref, f32[1,2048]{1,0:T(1,128)S(1)} %bitcast.12, ...), custom_call_target="tpu_custom_call" | custom-call | flops 400000000 | bytes 1048576 | tf_op jit(solution)/shard_map/rest_heads/pallas_call | solution.py:194
  34.5 36.1 %all_to_all.5.all_ref = bf16[64,16,256]{2,1,0:T(8,128)(2,1)S(1)} all-to-all(bf16[64,16,256]{2,1,0:T(8,128)(2,1)S(1)} %get-tuple-element.23), channel_id=1, replica_groups=mesh['sp'=64,'dp_0'=4,'dp_1'=2] {'sp'}, dimensions={0} | all-to-all | bytes 1048576 | tf_op jit(solution)/shard_map/all_to_all | solution.py:243
  70.6 1.3 %carry_in.1 = bf16[128,2048]{1,0:T(8,128)(2,1)} custom-call(bf16[64,16,256]{2,1,0:T(8,128)(2,1)S(1)} %all_to_all.5.all_ref, f32[2,128,256]{2,1,0:T(8,128)S(1)} %get-tuple-element.24.refs_0_, f32[2,128,256]{2,1,0:T(8,128)S(1)} %get-tuple-element.25.refs_1_, f32[2,2,8,256]{3,2,1,0:T(8,128)S(1)} %get-tuple-element.26.refs_2_, ...), custom_call_target="tpu_custom_call" | custom-call | flops 400000000 | bytes 1048576 | tf_op jit(solution)/shard_map/carry_in/pallas_call | solution.py:194
  (1 shorter events, 0.0 us)
Async XLA Ops:
  0.0 5.9 %copy-start.4 = (bf16[2,1,256,256]{3,2,1,0:T(8,128)(2,1)S(1)}, bf16[2,1,256,256]{3,2,1,0:T(8,128)(2,1)}, u32[]{:S(2)}) copy-start(bf16[2,1,256,256]{3,2,1,0:T(8,128)(2,1)} %param.7) | copy-start | bytes 786436
  0.0 25.7 %copy-start = (bf16[1,128,2048]{2,1,0:T(8,128)(2,1)S(1)}, bf16[1,128,2048]{2,1,0:T(8,128)(2,1)}, u32[]{:S(2)}) copy-start(bf16[1,128,2048]{2,1,0:T(8,128)(2,1)} %param.5) | copy-start | bytes 1572868
  2.5 20.8 %collective-permute-start.1 = (bf16[2,2,256,256]{3,2,1,0:T(8,128)(2,1)S(1)}, bf16[2,2,256,256]{3,2,1,0:T(8,128)(2,1)S(1)}, u32[]{:S(2)}, u32[]{:S(2)}) collective-permute-start(bf16[2,2,256,256]{3,2,1,0:T(8,128)(2,1)S(1)} %bitcast.7), channel_id=1, source_target_pairs={{0,2},{1,7},{2,4},{3,1},{4,6},{5,3},{6,0},{7,5},{8,10},{9,15},{10,... | collective-permute-start | bytes 1572872 | tf_op jit(solution)/shard_map/ppermute | solution.py:218
  5.9 25.6 %copy-start.1 = (f32[1,8192]{1,0:T(1,128)S(1)}, f32[1,8192]{1,0:T(1,128)}, u32[]{:S(2)}) copy-start(f32[1,8192]{1,0:T(1,128)} %pace_ref.1) | copy-start | bytes 98308
  5.9 25.6 %copy-start.2 = (bf16[4,2048]{1,0:T(4,128)(2,1)S(1)}, bf16[4,2048]{1,0:T(4,128)(2,1)}, u32[]{:S(2)}) copy-start(bf16[4,2048]{1,0:T(4,128)(2,1)} %cw_ref.1) | copy-start | bytes 49156
  5.9 25.6 %copy-start.3 = (f32[2048]{0:T(1024)S(1)}, f32[2048]{0:T(1024)}, u32[]{:S(2)}) copy-start(f32[2048]{0:T(1024)} %param.8) | copy-start | bytes 24580
  6.0 15.4 %collective-permute-start.3 = (bf16[2,256,256]{2,1,0:T(8,128)(2,1)S(1)}, bf16[2,256,256]{2,1,0:T(8,128)(2,1)S(1)}, u32[]{:S(2)}, u32[]{:S(2)}) collective-permute-start(bf16[2,256,256]{2,1,0:T(8,128)(2,1)S(1)} %bitcast.13), channel_id=1, source_target_pairs={{0,4},{2,6},{4,0},{6,2},{1,5},{3,7},{5,1},{7,3},{8,12},{10,14},{12... | collective-permute-start | bytes 786440 | tf_op jit(solution)/shard_map/ppermute | solution.py:221
  21.4 12.1 %collective-permute-start.4 = (bf16[2,256,256]{2,1,0:T(8,128)(2,1)S(1)}, bf16[2,256,256]{2,1,0:T(8,128)(2,1)S(1)}, u32[]{:S(2)}, u32[]{:S(2)}) collective-permute-start(bf16[2,256,256]{2,1,0:T(8,128)(2,1)S(1)} %collective-permute-done.3.wb_ref), channel_id=1, source_target_pairs={{0,1},{1,0},{2,3},{3,2},{4,5},{5,4},{6,7},{7,6},{8,9},{9,8},{10,11... | collective-permute-start | bytes 786440 | tf_op jit(solution)/shard_map/ppermute | solution.py:230
  23.3 10.2 %collective-permute-start.2 = (bf16[2,2,256,256]{3,2,1,0:T(8,128)(2,1)S(1)}, bf16[2,2,256,256]{3,2,1,0:T(8,128)(2,1)S(1)}, u32[]{:S(2)}, u32[]{:S(2)}) collective-permute-start(bf16[2,2,256,256]{3,2,1,0:T(8,128)(2,1)S(1)} %collective-permute-done.1.wa_ref), channel_id=1, source_target_pairs={{0,1},{1,0},{2,3},{3,2},{4,5},{5,4},{6,7},{7,6},{8,9},{9,8},{10,11... | collective-permute-start | bytes 1572872 | tf_op jit(solution)/shard_map/ppermute | solution.py:229
  25.8 5.8 %collective-permute-start = (bf16[8,2048]{1,0:T(8,128)(2,1)S(1)}, bf16[8,2048]{1,0:T(8,128)(2,1)S(1)}, u32[]{:S(2)}, u32[]{:S(2)}) collective-permute-start(bf16[8,2048]{1,0:T(8,128)(2,1)S(1)} %slice_bitcast_fusion), channel_id=1, source_target_pairs={{0,8},{8,16},{16,24},{24,32},{32,40},{40,48},{48,56},{56,64},{64,7... | collective-permute-start | bytes 98312 | tf_op jit(solution)/shard_map/ppermute | solution.py:222

commit v2 on v1

v2 whole, which is shorter than its diff:
```python
import jax
import jax.numpy as jnp
from jax import lax
from jax.experimental import pallas as pl
from jax.experimental.pallas import tpu as pltpu
from jax.sharding import Mesh
from jax.sharding import PartitionSpec as P

HEADS = 8
BLOCK = 256
CONV = 4
ROWS = 128
CHUNKS = 8
STEPS = ROWS // CHUNKS
LANES = 128

gate_power = 8.0
f32, bf16 = jnp.float32, jnp.bfloat16


def order_matrix(transposed):
    here = lax.broadcasted_iota(jnp.int32, (ROWS, ROWS), 1 if transposed else 0)
    position = lax.broadcasted_iota(jnp.int32, (ROWS, ROWS), 0 if transposed else 1)
    return position == (here & (CHUNKS - 1)) * STEPS + (here >> 3)


def softplus_of_minus(rate):
    e = jnp.exp(-jnp.abs(rate))
    series = e * (1 - e * (1 / 2 - e * (1 / 3 - e * (1 / 4 - e * (1 / 5 - e * (1 / 6))))))
    return jnp.maximum(-rate, 0.0) + jnp.where(e < 0.05, series, jnp.log(1.0 + e))


def sublane_before(tile, shift, fill):
    row = lax.broadcasted_iota(jnp.int32, tile.shape, 0)
    return jnp.where(row < shift, fill, pltpu.roll(tile, shift, 0))


def conv_all(x_ref, halo_ref, cw_ref, cv_ref):
    perm = order_matrix(False).astype(bf16)
    for h in range(HEADS):
        cols = pl.ds(h * BLOCK, BLOCK)
        moved = jnp.dot(perm, x_ref[:, cols], preferred_element_type=f32)
        step = [moved[CHUNKS * r : CHUNKS * (r + 1)] for r in range(STEPS)]
        halo = halo_ref[:, cols].astype(f32)
        taps = cw_ref[:, cols].astype(f32)
        early = [
            sublane_before(step[STEPS - j], 1, halo[8 - j : 9 - j]) for j in (3, 2, 1)
        ]
        line = early + step
        for r in range(0, STEPS, 2):
            both = []
            for q in (r, r + 1):
                total = taps[0:1] * line[q]
                for tap in range(1, CONV):
                    total = total + taps[tap : tap + 1] * line[q + tap]
                both.append(total)
            cv_ref[pl.ds(CHUNKS * r, 2 * CHUNKS), cols] = jnp.concatenate(both, 0).astype(bf16)


def one_head(head, cv_ref, w0, w1, pace_ref, rate_ref, pre_ref, h_ref, p_ref, edge_ref, slot):
    cols = pl.ds(pl.multiple_of(head * BLOCK, BLOCK), BLOCK)
    values = cv_ref[:, cols]
    pre_ref[0] = jnp.dot(values, w0, preferred_element_type=f32)
    pre_ref[1] = jnp.dot(values, w1, preferred_element_type=f32)
    pre_ref[2] = values.astype(f32)
    soft = gate_power * softplus_of_minus(rate_ref[:, cols])
    totals = []
    for lane in range(0, BLOCK, LANES):
        at = slice(lane, lane + LANES)
        soft_here = soft[:, at]
        state = run = used = None
        for r in range(STEPS):
            rows = slice(CHUNKS * r, CHUNKS * (r + 1))
            x0 = pre_ref[0, rows, at].astype(bf16).astype(f32)
            x1 = pre_ref[1, rows, at].astype(bf16).astype(f32)
            recur_gate = 1.0 / (1.0 + jnp.exp(-x0))
            input_gate = 1.0 / (1.0 + jnp.exp(-x1))
            loss = pace_ref[rows, :] * recur_gate * soft_here
            decay = jnp.exp(-loss)
            v = 2.0 * loss
            series = v * (1 - v * (1 / 2 - v * (1 / 6 - v * (1 / 24 - v * (1 / 120)))))
            gone = jnp.where(v < 0.1, series, 1.0 - decay * decay)
            drive = jnp.sqrt(gone) * input_gate * pre_ref[2, rows, at]
            if r == 0:
                state, run, used = drive, decay, loss
            else:
                state, run, used = decay * state + drive, decay * run, used + loss
            h_ref[slot, rows, at] = state
            p_ref[slot, rows, at] = run
        for shift in (1, 2, 4):
            state = state + run * sublane_before(state, shift, 0.0)
            run = run * sublane_before(run, shift, 1.0)
        edge_ref[slot, 0, :, at] = sublane_before(state, 1, 0.0)
        edge_ref[slot, 1, :, at] = sublane_before(run, 1, 1.0)
        totals.append((jnp.sum(used, 0, keepdims=True), state[CHUNKS - 1 : CHUNKS]))
    return tuple(jnp.concatenate([t[k] for t in totals], 1) for k in (0, 1))


def place():
    x, c = lax.axis_index("dp_0"), lax.axis_index("dp_1")
    return x, c, (x + 3 + 2 * c) & 3, (x + 1 + 2 * c) & 3, (x + 2) & 3


def heads_of(group):
    x, c, first, second, far = place()
    return {
        "own": [2 * x + c, 2 * first + c, 2 * second + c],
        "mid": [2 * far + c, 2 * x + 1 - c, 2 * second + 1 - c, 2 * first + 1 - c],
        "end": [2 * far + 1 - c],
    }[group]


def own_kernel(x_ref, halo_ref, cw_ref, rate_ref, pace_ref, own_ref, first_ref, second_ref, cv_ref, pcol_ref, pass_ref, h_ref, p_ref, edge_ref, tot_ref, pre_ref):
    here = lax.axis_index("z") * lax.axis_size("y") + lax.axis_index("y")
    pace = pace_ref[:, pl.ds(pl.multiple_of(here * ROWS, ROWS), ROWS)]
    column = jnp.sum(jnp.where(order_matrix(False), pace, 0.0), axis=1, keepdims=True)
    pcol_ref[...] = jnp.broadcast_to(column, (ROWS, LANES))
    conv_all(x_ref, halo_ref, cw_ref, cv_ref)
    maps = (own_ref, first_ref, second_ref)
    for slot, head in enumerate(heads_of("own")):
        pass_ref[slot] = maps[slot][...]
        used, state = one_head(head, cv_ref, maps[slot][0], maps[slot][1], pcol_ref, rate_ref, pre_ref, h_ref, p_ref, edge_ref, slot)
        tot_ref[0, slot : slot + 1] = used
        tot_ref[1, slot : slot + 1] = state


def mid_kernel(cv_ref, pcol_ref, rate_ref, far_ref, swap_ref, h_ref, p_ref, edge_ref, tot_ref, pre_ref):
    for slot, head in enumerate(heads_of("mid")):
        w = far_ref if slot == 0 else swap_ref.at[slot - 1]
        used, state = one_head(head, cv_ref, w[0], w[1], pcol_ref, rate_ref, pre_ref, h_ref, p_ref, edge_ref, slot)
        tot_ref[0, slot : slot + 1] = used
        tot_ref[1, slot : slot + 1] = state


def end_kernel(cv_ref, pcol_ref, rate_ref, w_ref, own_ref, mid_ref, h_ref, p_ref, edge_ref, send_ref, pre_ref):
    (head,) = heads_of("end")
    totals = one_head(head, cv_ref, w_ref[0], w_ref[1], pcol_ref, rate_ref, pre_ref, h_ref, p_ref, edge_ref, 0)
    lines = []
    for k in (0, 1):
        lines += [own_ref[k], mid_ref[k], totals[k]]
    message = jnp.concatenate(lines, 0).astype(bf16)
    for j in range(send_ref.shape[0]):
        send_ref[j] = message


def row_kernel(all_ref, send_ref):
    used = state = None
    for j in range(all_ref.shape[0]):
        line = all_ref[j].astype(f32)
        if j == 0:
            used, state = line[:HEADS], line[HEADS:]
        else:
            used, state = used + line[:HEADS], jnp.exp(-line[:HEADS]) * state + line[HEADS:]
    message = jnp.concatenate([used, state], 0).astype(bf16)
    for j in range(send_ref.shape[0]):
        send_ref[j] = message


def before(all_ref, here, state):
    for j in range(all_ref.shape[0]):
        line = all_ref[j].astype(f32)
        mine = (j < here).astype(f32)
        drive = line[HEADS:] * mine
        state = drive if state is None else jnp.exp(-(line[:HEADS] * mine)) * state + drive
    return state


def last_kernel(row_ref, column_ref, *refs):
    groups, out_ref = refs[:9], refs[9]
    carried = before(column_ref, lax.axis_index("z"), None)
    carried = before(row_ref, lax.axis_index("y"), carried)
    back = order_matrix(True).astype(bf16)
    at = 0
    for g, name in enumerate(("own", "mid", "end")):
        h_ref, p_ref, edge_ref = groups[3 * g : 3 * g + 3]
        for slot, head in enumerate(heads_of(name)):
            enters = edge_ref[slot, 0] + edge_ref[slot, 1] * carried[at : at + 1]
            whole = h_ref[slot].reshape(STEPS, CHUNKS, BLOCK) + p_ref[slot].reshape(
                STEPS, CHUNKS, BLOCK
            ) * enters.reshape(1, CHUNKS, BLOCK)
            rounded = whole.reshape(ROWS, BLOCK).astype(bf16)
            cols = pl.ds(pl.multiple_of(head * BLOCK, BLOCK), BLOCK)
            out_ref[:, cols] = jnp.dot(back, rounded, preferred_element_type=f32).astype(bf16)
            at += 1


def vmem(count):
    return [pl.BlockSpec(memory_space=pltpu.VMEM)] * count


def call(kernel, outs, args, scratch=True, us=2.0):
    return pl.pallas_call(
        kernel,
        out_shape=[jax.ShapeDtypeStruct(s, d) for s, d in outs],
        in_specs=vmem(len(args)),
        out_specs=vmem(len(outs)),
        scratch_shapes=[pltpu.VMEM((3, ROWS, BLOCK), f32)] if scratch else [],
        compiler_params=pltpu.CompilerParams(vmem_limit_bytes=16 * 2**20),
        cost_estimate=pl.CostEstimate(
            flops=int(us * 2e8), bytes_accessed=1 << 20, transcendentals=1 << 18
        ),
    )(*args)


def head_outs(n):
    return [((n, ROWS, BLOCK), f32), ((n, ROWS, BLOCK), f32), ((n, 2, CHUNKS, BLOCK), f32)]


def layer(inputs, conv_weight, gate_weight, rate_param, pace):
    x = inputs[0]
    rate = rate_param[None]
    columns, lines = lax.axis_size("z"), lax.axis_size("y")
    dp, sp = ("dp_0", "dp_1"), ("z", "y")

    def along(array, way):
        pairs = [(2 * i + c, 2 * ((i + (way, -way)[c]) % 4) + c) for i in range(4) for c in (0, 1)]
        return lax.ppermute(array, dp, pairs)

    def swapped(array):
        return lax.ppermute(array, "dp_1", [(0, 1), (1, 0)])

    own = gate_weight[:, 0]
    first = along(own, 1)
    second = along(own, -1)
    halo = lax.ppermute(x[ROWS - 8 :], sp, [(i, i + 1) for i in range(columns * lines - 1)])
    far = along(first, 1)
    cv, pcol, ours, *own_out, own_tot = call(
        own_kernel,
        [
            ((ROWS, HEADS * BLOCK), bf16),
            ((ROWS, LANES), f32),
            ((3, 2, BLOCK, BLOCK), bf16),
            *head_outs(3),
            ((2, 3, BLOCK), f32),
        ],
        (x, halo, conv_weight, rate, pace, own, first, second),
    )
    theirs = swapped(ours)
    far_theirs = swapped(far)
    *mid_out, mid_tot = call(mid_kernel, [*head_outs(4), ((2, 4, BLOCK), f32)], (cv, pcol, rate, far, theirs))
    message = ((lines, 2 * HEADS, BLOCK), bf16)
    *end_out, send = call(end_kernel, [*head_outs(1), message], (cv, pcol, rate, far_theirs, own_tot, mid_tot))
    row = lax.all_to_all(send, "y", split_axis=0, concat_axis=0, tiled=True)
    (send,) = call(row_kernel, [((columns, 2 * HEADS, BLOCK), bf16)], (row,), scratch=False)
    column = lax.all_to_all(send, "z", split_axis=0, concat_axis=0, tiled=True)
    (result,) = call(
        last_kernel, [((ROWS, HEADS * BLOCK), bf16)], (row, column, *own_out, *mid_out, *end_out), scratch=False
    )
    return result[None]


def solution(mesh):
    axes = ("z", "y", "dp_0", "dp_1")
    finer = Mesh(mesh.devices.reshape(mesh.shape["sp"] // 8, 8, 4, 2), axes)
    dp, sp = ("dp_0", "dp_1"), ("z", "y")
    in_specs = (P(dp, sp, None), P(), P(None, dp, None, None), P(), P(dp, None))
    out_specs = P(dp, sp, None)
    return jax.shard_map(layer, mesh=finer, in_specs=in_specs, out_specs=out_specs, check_vma=False)
```

time: 72.2 us -> 68 us (0.942)
  blocking collectives: 38.6 us -> 30.8 us
  local copies, waits for them, and re-layouts: 0.03 us -> 2.76 us
    all_to_all x1 -> x2, blocking collectives: 36.1 us -> 30.8 us  [the longest x1 18.5 us: layer(): column = lax.all_to_all(send, 'z', split_axis=0, concat_axis=0, tiled=True)]
    all_gather x1 -> x0, blocking collectives: 2.51 us -> none  [body(): pair = lax.all_gather(own, 'dp_1')]
    unnamed x10, local copies, waits for them, and re-layouts: 0.03 us -> 2 us
    slice x1, local copies, waits for them, and re-layouts: 0.01 us -> 0.76 us  [layer(): x[ROWS - 8:]]
    ppermute x5 -> x6, starting transfers between devices: 16 us -> 16.4 us  [the longest x3 9.11 us: along(): return lax.ppermute(array, dp, pairs)]
    ppermute x5 -> x6, waiting for transfers between devices: 13 us -> 13.4 us  [the longest x3 7.55 us: along(): return lax.ppermute(array, dp, pairs)]
    pallas_call x4 -> x5, Pallas kernels: 4.16 us -> 4.04 us  [call(): pl.pallas_call(kernel, out_shape=[jax.ShapeDtypeStruct(s, d) for s, d in...]
  transfers between devices with their start and end apart: 5 -> 6, of which waited for: 2 -> 3; matrix products, arithmetic and copies ran while one was open for 0% -> 1% of each run, Pallas kernels for 3% -> 2%
where the time goes in v2:
time: 68 us; the launch traced here: 67.5 us
  blocking collectives  30.8 us (45%)
  starting transfers between devices  16.4 us (24%)
  waiting for transfers between devices  13.4 us (20%)
  Pallas kernels  4.04 us (6%)
  local copies, waits for them, and re-layouts  2.76 us (4%)
    all_to_all x1, blocking collectives, layer(): column = lax.all_to_all(send, 'z', split_axis=0, concat_axis=0, tiled=True)  18.5 us
    all_to_all x1, blocking collectives, layer(): row = lax.all_to_all(send, 'y', split_axis=0, concat_axis=0, tiled=True)  12.3 us
    ppermute x3, starting transfers between devices, along(): return lax.ppermute(array, dp, pairs)  9.11 us
    ppermute x3, waiting for transfers between devices, along(): return lax.ppermute(array, dp, pairs)  7.55 us
    ppermute x1, waiting for transfers between devices, layer(): lax.ppermute(x[ROWS - 8:], sp, [(i, i + 1) for i in range(columns * lines...  5.46 us
    pallas_call x5, Pallas kernels, call(): pl.pallas_call(kernel, out_shape=[jax.ShapeDtypeStruct(s, d) for s, d in...  4.04 us
    ppermute x2, starting transfers between devices, swapped(): return lax.ppermute(array, 'dp_1', [(0, 1), (1, 0)])  3.83 us
    ppermute x1, starting transfers between devices, layer(): lax.ppermute(x[ROWS - 8:], sp, [(i, i + 1) for i in range(columns * lines...  3.47 us
  transfers between devices with their start and end apart: 6, of which 3 were waited for; matrix products, arithmetic and copies ran while one was open for 1% of the time, Pallas kernels for 2%

profile of v2, /device:TPU:8, one launch (start us, length us, event | category | flops | bytes accessed | tf_op | source)
XLA Modules:
  0.0 67.5 jit_solution(1560702658241231486)
XLA Ops:
  0.0 0.0 copy-start
  0.0 0.0 copy-start.3
  0.0 0.0 copy-start.4
  0.0 3.5 %collective-permute-start.1 = (bf16[2,256,256]{2,1,0:T(8,128)(2,1)}, bf16[2,256,256]{2,1,0:T(8,128)(2,1)S(1)}, u32[]{:S(2)}, u32[]{:S(2)}) collective-permute-start(bf16[2,256,256]{2,1,0:T(8,128)(2,1)} %bitcast.10), channel_id=1, source_target_pairs={{0,2},{1,7},{2,4},{3,1},{4,6},{5,3},{6,0},{7,5},{8,10},{9,15},{10,... | collective-permute-start | bytes 786440 | tf_op jit(solution)/shard_map/ppermute | solution.py:217
  3.6 3.7 %collective-permute-start.2 = (bf16[2,256,256]{2,1,0:T(8,128)(2,1)}, bf16[2,256,256]{2,1,0:T(8,128)(2,1)S(1)}, u32[]{:S(2)}, u32[]{:S(2)}) collective-permute-start(bf16[2,256,256]{2,1,0:T(8,128)(2,1)} %bitcast.11), channel_id=1, source_target_pairs={{0,6},{1,3},{2,0},{3,5},{4,2},{5,7},{6,4},{7,1},{8,14},{9,11},{10,... | collective-permute-start | bytes 786440 | tf_op jit(solution)/shard_map/ppermute | solution.py:217
  7.2 0.8 %slice_bitcast_fusion = bf16[8,2048]{1,0:T(8,128)(2,1)S(1)} fusion(bf16[1,128,2048]{2,1,0:T(8,128)(2,1)} %param.5), kind=kLoop, calls=%fused_computation | loop fusion | bytes 65536 | tf_op jit(solution)/shard_map/slice | solution.py:225
  8.0 3.5 %collective-permute-start = (bf16[8,2048]{1,0:T(8,128)(2,1)S(1)}, bf16[8,2048]{1,0:T(8,128)(2,1)S(1)}, u32[]{:S(2)}, u32[]{:S(2)}) collective-permute-start(bf16[8,2048]{1,0:T(8,128)(2,1)S(1)} %slice_bitcast_fusion), channel_id=1, source_target_pairs={{0,8},{8,16},{16,24},{24,32},{32,40},{40,48},{48,56},{56,64},{64,7... | collective-permute-start | bytes 98312 | tf_op jit(solution)/shard_map/ppermute | solution.py:225
  11.5 5.5 %collective-permute-done.halo_ref = bf16[8,2048]{1,0:T(8,128)(2,1)S(1)} collective-permute-done((bf16[8,2048]{1,0:T(8,128)(2,1)S(1)}, bf16[8,2048]{1,0:T(8,128)(2,1)S(1)}, u32[]{:S(2)}, u32[]{:S(2)}) %collective-permute-start) | collective-permute-done | bytes 32800 | tf_op jit(solution)/shard_map/ppermute | solution.py:225
  16.9 0.0 collective-permute-done.1.first_ref
  16.9 0.0 collective-permute-done.2.second_ref
  16.9 0.0 copy-done
  16.9 0.0 copy-done.3
  16.9 0.0 copy-done.4
  16.9 0.0 copy-start.1
  17.0 1.0 %copy-done.1 = bf16[1,128,2048]{2,1,0:T(8,128)(2,1)S(1)} copy-done((bf16[1,128,2048]{2,1,0:T(8,128)(2,1)S(1)}, bf16[1,128,2048]{2,1,0:T(8,128)(2,1)}, u32[]{:S(2)}) %copy-start.1) | copy-done | bytes 524312
  18.0 0.0 copy-start.2
  18.0 0.9 %copy-done.2 = bf16[2,1,256,256]{3,2,1,0:T(8,128)(2,1)S(1)} copy-done((bf16[2,1,256,256]{3,2,1,0:T(8,128)(2,1)S(1)}, bf16[2,1,256,256]{3,2,1,0:T(8,128)(2,1)}, u32[]{:S(2)}) %copy-start.2) | copy-done | bytes 262168
  18.9 1.3 %shard_map.55 = (bf16[128,2048]{1,0:T(8,128)(2,1)S(1)}, f32[128,128]{1,0:T(8,128)S(1)}, bf16[3,2,256,256]{3,2,1,0:T(8,128)(2,1)S(1)}, f32[3,128,256]{2,1,0:T(8,1...) custom-call(bf16[128,2048]{1,0:T(8,128)(2,1)S(1)} %bitcast.9, ...), custom_call_target="tpu_custom_call" | custom-call | flops 400000000 | bytes 1048576 | tf_op jit(solution)/shard_map/pallas_call | solution.py:192
  20.3 1.9 %collective-permute-start.5 = (bf16[3,2,256,256]{3,2,1,0:T(8,128)(2,1)S(1)}, bf16[3,2,256,256]{3,2,1,0:T(8,128)(2,1)S(1)}, u32[]{:S(2)}, u32[]{:S(2)}) collective-permute-start(bf16[3,2,256,256]{3,2,1,0:T(8,128)(2,1)S(1)} %get-tuple-element.23), channel_id=1, source_target_pairs={{0,1},{1,0},{2,3},{3,2},{4,5},{5,4},{6,7},{7,6},{8,9},{9,8},{10,11... | collective-permute-start | bytes 2359304 | tf_op jit(solution)/shard_map/ppermute | solution.py:220
  22.2 1.9 %collective-permute-start.3 = (bf16[2,256,256]{2,1,0:T(8,128)(2,1)S(1)}, bf16[2,256,256]{2,1,0:T(8,128)(2,1)S(1)}, u32[]{:S(2)}, u32[]{:S(2)}) collective-permute-start(bf16[2,256,256]{2,1,0:T(8,128)(2,1)S(1)} %collective-permute-done.1.first_ref), channel_id=1, source_target_pairs={{0,2},{1,7},{2,4},{3,1},{4,6},{5,3},{6,0},{7,5},{8,10},{9,15},{10,... | collective-permute-start | bytes 786440 | tf_op jit(solution)/shard_map/ppermute | solution.py:217
  24.1 7.5 %collective-permute-done.3.far_ref = bf16[2,256,256]{2,1,0:T(8,128)(2,1)S(1)} collective-permute-done((bf16[2,256,256]{2,1,0:T(8,128)(2,1)S(1)}, bf16[2,256,256]{2,1,0:T(8,128)(2,1)S(1)}, u32[]{:S(2)}, u32[]{:S(2)}) %collective-permute-start.3) | collective-permute-done | bytes 262176 | tf_op jit(solution)/shard_map/ppermute | solution.py:217
  31.7 1.9 %collective-permute-start.4 = (bf16[2,256,256]{2,1,0:T(8,128)(2,1)S(1)}, bf16[2,256,256]{2,1,0:T(8,128)(2,1)S(1)}, u32[]{:S(2)}, u32[]{:S(2)}) collective-permute-start(bf16[2,256,256]{2,1,0:T(8,128)(2,1)S(1)} %collective-permute-done.3.far_ref), channel_id=1, source_target_pairs={{0,1},{1,0},{2,3},{3,2},{4,5},{5,4},{6,7},{7,6},{8,9},{9,8},{10,11... | collective-permute-start | bytes 786440 | tf_op jit(solution)/shard_map/ppermute | solution.py:220
  33.6 0.0 collective-permute-done.5.swap_ref
  33.6 1.1 %shard_map.56 = (f32[4,128,256]{2,1,0:T(8,128)S(1)}, f32[4,128,256]{2,1,0:T(8,128)S(1)}, f32[4,2,8,256]{3,2,1,0:T(8,128)S(1)}, f32[2,4,256]{2,1,0:T(4,128)S(1)}) custom-call(bf16[128,2048]{1,0:T(8,128)(2,1)S(1)} %get-tuple-element.20.cv_ref, f32[128,128]{1,0:T(8,128)S(1)} %get-tuple-element.21.pcol_ref, f32[1,2048]{1,0:T(1,128)S(1)} %bitcast.7, ...), custom_call_target="tpu_custom_call" | custom-call | flops 400000000 | bytes 1048576 | tf_op jit(solution)/shard_map/pallas_call | solution.py:192
  34.7 0.4 collective-permute-done.4.w_ref
  35.1 0.4 shard_map.57
  35.5 12.3 %all_to_all.10.all_ref.row_ref = bf16[8,16,256]{2,1,0:T(8,128)(2,1)S(1)} all-to-all(bf16[8,16,256]{2,1,0:T(8,128)(2,1)S(1)} %get-tuple-element.25), channel_id=1, replica_groups=mesh['z'=8,'y'=8,'dp_0'=4,'dp_1'=2] {'y'}, dimensions={0} | all-to-all | bytes 131072 | tf_op jit(solution)/shard_map/all_to_all | solution.py:243
  47.8 18.5 %all_to_all.11.column_ref = bf16[8,16,256]{2,1,0:T(8,128)(2,1)S(1)} all-to-all(bf16[8,16,256]{2,1,0:T(8,128)(2,1)S(1)} %shard_map.58), channel_id=1, replica_groups=mesh['z'=8,'y'=8,'dp_0'=4,'dp_1'=2] {'z'}, dimensions={0} | all-to-all | bytes 131072 | tf_op jit(solution)/shard_map/all_to_all | solution.py:245
  66.3 1.2 %shard_map.59 = bf16[128,2048]{1,0:T(8,128)(2,1)} custom-call(bf16[8,16,256]{2,1,0:T(8,128)(2,1)S(1)} %all_to_all.10.all_ref.row_ref, bf16[8,16,256]{2,1,0:T(8,128)(2,1)S(1)} %all_to_all.11.column_ref, f32[3,128,256]{2,1,0:T(8,128)S(1)} %get-tuple-element.26.refs_0_, f32[3,128,256]{2,1,0:T(8,128)S(1)} %get-tuple-element.27.refs_1_, ...), custom_call_target="tpu_custom_call" | custom-call | flops 400000000 | bytes 1048576 | tf_op jit(solution)/shard_map/pallas_call | solution.py:192
  (1 shorter events, 0.0 us)
Async XLA Ops:
  0.0 16.9 %copy-start = (f32[2048]{0:T(1024)S(1)}, f32[2048]{0:T(1024)}, u32[]{:S(2)}) copy-start(f32[2048]{0:T(1024)} %param.8) | copy-start | bytes 24580
  0.0 16.9 %copy-start.3 = (f32[1,8192]{1,0:T(1,128)S(1)}, f32[1,8192]{1,0:T(1,128)}, u32[]{:S(2)}) copy-start(f32[1,8192]{1,0:T(1,128)} %pace_ref.1) | copy-start | bytes 98308
  0.0 16.9 %copy-start.4 = (bf16[4,2048]{1,0:T(4,128)(2,1)S(1)}, bf16[4,2048]{1,0:T(4,128)(2,1)}, u32[]{:S(2)}) copy-start(bf16[4,2048]{1,0:T(4,128)(2,1)} %cw_ref.1) | copy-start | bytes 49156
  0.0 16.9 %collective-permute-start.1 = (bf16[2,256,256]{2,1,0:T(8,128)(2,1)}, bf16[2,256,256]{2,1,0:T(8,128)(2,1)S(1)}, u32[]{:S(2)}, u32[]{:S(2)}) collective-permute-start(bf16[2,256,256]{2,1,0:T(8,128)(2,1)} %bitcast.10), channel_id=1, source_target_pairs={{0,2},{1,7},{2,4},{3,1},{4,6},{5,3},{6,0},{7,5},{8,10},{9,15},{10,... | collective-permute-start | bytes 786440 | tf_op jit(solution)/shard_map/ppermute | solution.py:217
  3.6 13.4 %collective-permute-start.2 = (bf16[2,256,256]{2,1,0:T(8,128)(2,1)}, bf16[2,256,256]{2,1,0:T(8,128)(2,1)S(1)}, u32[]{:S(2)}, u32[]{:S(2)}) collective-permute-start(bf16[2,256,256]{2,1,0:T(8,128)(2,1)} %bitcast.11), channel_id=1, source_target_pairs={{0,6},{1,3},{2,0},{3,5},{4,2},{5,7},{6,4},{7,1},{8,14},{9,11},{10,... | collective-permute-start | bytes 786440 | tf_op jit(solution)/shard_map/ppermute | solution.py:217
  8.0 8.9 %collective-permute-start = (bf16[8,2048]{1,0:T(8,128)(2,1)S(1)}, bf16[8,2048]{1,0:T(8,128)(2,1)S(1)}, u32[]{:S(2)}, u32[]{:S(2)}) collective-permute-start(bf16[8,2048]{1,0:T(8,128)(2,1)S(1)} %slice_bitcast_fusion), channel_id=1, source_target_pairs={{0,8},{8,16},{16,24},{24,32},{32,40},{40,48},{48,56},{56,64},{64,7... | collective-permute-start | bytes 98312 | tf_op jit(solution)/shard_map/ppermute | solution.py:225
  16.9 1.0 %copy-start.1 = (bf16[1,128,2048]{2,1,0:T(8,128)(2,1)S(1)}, bf16[1,128,2048]{2,1,0:T(8,128)(2,1)}, u32[]{:S(2)}) copy-start(bf16[1,128,2048]{2,1,0:T(8,128)(2,1)} %param.5) | copy-start | bytes 1572868
  18.0 0.9 %copy-start.2 = (bf16[2,1,256,256]{3,2,1,0:T(8,128)(2,1)S(1)}, bf16[2,1,256,256]{3,2,1,0:T(8,128)(2,1)}, u32[]{:S(2)}) copy-start(bf16[2,1,256,256]{3,2,1,0:T(8,128)(2,1)} %param.7) | copy-start | bytes 786436
  20.3 13.3 %collective-permute-start.5 = (bf16[3,2,256,256]{3,2,1,0:T(8,128)(2,1)S(1)}, bf16[3,2,256,256]{3,2,1,0:T(8,128)(2,1)S(1)}, u32[]{:S(2)}, u32[]{:S(2)}) collective-permute-start(bf16[3,2,256,256]{3,2,1,0:T(8,128)(2,1)S(1)} %get-tuple-element.23), channel_id=1, source_target_pairs={{0,1},{1,0},{2,3},{3,2},{4,5},{5,4},{6,7},{7,6},{8,9},{9,8},{10,11... | collective-permute-start | bytes 2359304 | tf_op jit(solution)/shard_map/ppermute | solution.py:220
  22.2 9.5 %collective-permute-start.3 = (bf16[2,256,256]{2,1,0:T(8,128)(2,1)S(1)}, bf16[2,256,256]{2,1,0:T(8,128)(2,1)S(1)}, u32[]{:S(2)}, u32[]{:S(2)}) collective-permute-start(bf16[2,256,256]{2,1,0:T(8,128)(2,1)S(1)} %collective-permute-done.1.first_ref), channel_id=1, source_target_pairs={{0,2},{1,7},{2,4},{3,1},{4,6},{5,3},{6,0},{7,5},{8,10},{9,15},{10,... | collective-permute-start | bytes 786440 | tf_op jit(solution)/shard_map/ppermute | solution.py:217
  31.7 3.4 %collective-permute-start.4 = (bf16[2,256,256]{2,1,0:T(8,128)(2,1)S(1)}, bf16[2,256,256]{2,1,0:T(8,128)(2,1)S(1)}, u32[]{:S(2)}, u32[]{:S(2)}) collective-permute-start(bf16[2,256,256]{2,1,0:T(8,128)(2,1)S(1)} %collective-permute-done.3.far_ref), channel_id=1, source_target_pairs={{0,1},{1,0},{2,3},{3,2},{4,5},{5,4},{6,7},{7,6},{8,9},{9,8},{10,11... | collective-permute-start | bytes 786440 | tf_op jit(solution)/shard_map/ppermute | solution.py:220

commit v3 on v2

--- a/solution.py
+++ b/solution.py
@@ -14,6 +14,7 @@
 STEPS = ROWS // CHUNKS
 LANES = 128
 
+
 gate_power = 8.0
 f32, bf16 = jnp.float32, jnp.bfloat16
 
@@ -35,12 +36,13 @@
     return jnp.where(row < shift, fill, pltpu.roll(tile, shift, 0))
 
 
-def conv_all(x_ref, halo_ref, cw_ref, cv_ref):
-    perm = order_matrix(False).astype(bf16)
+def conv_all(moved_ref, halo_ref, cw_ref, cv_ref):
     for h in range(HEADS):
         cols = pl.ds(h * BLOCK, BLOCK)
-        moved = jnp.dot(perm, x_ref[:, cols], preferred_element_type=f32)
-        step = [moved[CHUNKS * r : CHUNKS * (r + 1)] for r in range(STEPS)]
+        step = []
+        for r in range(0, STEPS, 2):
+            both = moved_ref[pl.ds(CHUNKS * r, 2 * CHUNKS), cols].astype(f32)
+            step += [both[:CHUNKS], both[CHUNKS:]]
         halo = halo_ref[:, cols].astype(f32)
         taps = cw_ref[:, cols].astype(f32)
         early = [
@@ -105,39 +107,49 @@
     x, c, first, second, far = place()
     return {
         "own": [2 * x + c, 2 * first + c, 2 * second + c],
-        "mid": [2 * far + c, 2 * x + 1 - c, 2 * second + 1 - c, 2 * first + 1 - c],
-        "end": [2 * far + 1 - c],
+        "rest": [2 * far, 2 * far + 1, 2 * x + 1 - c, 2 * second + 1 - c, 2 * first + 1 - c],
     }[group]
 
 
-def own_kernel(x_ref, halo_ref, cw_ref, rate_ref, pace_ref, own_ref, first_ref, second_ref, cv_ref, pcol_ref, pass_ref, h_ref, p_ref, edge_ref, tot_ref, pre_ref):
+def order_kernel(perm_ref):
+    perm_ref[...] = order_matrix(False).astype(bf16)
+
+
+def move_kernel(x_ref, perm_ref, moved_ref, tail_ref):
+    tail_ref[...] = x_ref[ROWS - 8 :]
+    perm = perm_ref[...]
+    for h in range(HEADS):
+        cols = pl.ds(h * BLOCK, BLOCK)
+        moved_ref[:, cols] = jnp.dot(perm, x_ref[:, cols], preferred_element_type=f32).astype(bf16)
+
+
+def conv_kernel(moved_ref, halo_ref, cw_ref, own_ref, first_ref, second_ref, cv_ref, pass_ref):
+    for slot, w in enumerate((own_ref, first_ref, second_ref)):
+        pass_ref[slot] = w[...]
+    conv_all(moved_ref, halo_ref, cw_ref, cv_ref)
+
+
+def own_kernel(cv_ref, rate_ref, pace_ref, own_ref, first_ref, second_ref, pcol_ref, h_ref, p_ref, edge_ref, tot_ref, pre_ref):
     here = lax.axis_index("z") * lax.axis_size("y") + lax.axis_index("y")
     pace = pace_ref[:, pl.ds(pl.multiple_of(here * ROWS, ROWS), ROWS)]
     column = jnp.sum(jnp.where(order_matrix(False), pace, 0.0), axis=1, keepdims=True)
     pcol_ref[...] = jnp.broadcast_to(column, (ROWS, LANES))
-    conv_all(x_ref, halo_ref, cw_ref, cv_ref)
     maps = (own_ref, first_ref, second_ref)
     for slot, head in enumerate(heads_of("own")):
-        pass_ref[slot] = maps[slot][...]
-        used, state = one_head(head, cv_ref, maps[slot][0], maps[slot][1], pcol_ref, rate_ref, pre_ref, h_ref, p_ref, edge_ref, slot)
-        tot_ref[0, slot : slot + 1] = used
-        tot_ref[1, slot : slot + 1] = state
-
-
-def mid_kernel(cv_ref, pcol_ref, rate_ref, far_ref, swap_ref, h_ref, p_ref, edge_ref, tot_ref, pre_ref):
-    for slot, head in enumerate(heads_of("mid")):
-        w = far_ref if slot == 0 else swap_ref.at[slot - 1]
+        w = maps[slot]
         used, state = one_head(head, cv_ref, w[0], w[1], pcol_ref, rate_ref, pre_ref, h_ref, p_ref, edge_ref, slot)
         tot_ref[0, slot : slot + 1] = used
         tot_ref[1, slot : slot + 1] = state
 
 
-def end_kernel(cv_ref, pcol_ref, rate_ref, w_ref, own_ref, mid_ref, h_ref, p_ref, edge_ref, send_ref, pre_ref):
-    (head,) = heads_of("end")
-    totals = one_head(head, cv_ref, w_ref[0], w_ref[1], pcol_ref, rate_ref, pre_ref, h_ref, p_ref, edge_ref, 0)
+def rest_kernel(cv_ref, pcol_ref, rate_ref, far_ref, swap_ref, own_ref, h_ref, p_ref, edge_ref, send_ref, pre_ref):
+    totals = []
+    for slot, head in enumerate(heads_of("rest")):
+        w = far_ref.at[slot] if slot < 2 else swap_ref.at[slot - 2]
+        totals.append(one_head(head, cv_ref, w[0], w[1], pcol_ref, rate_ref, pre_ref, h_ref, p_ref, edge_ref, slot))
     lines = []
     for k in (0, 1):
-        lines += [own_ref[k], mid_ref[k], totals[k]]
+        lines += [own_ref[k]] + [t[k] for t in totals]
     message = jnp.concatenate(lines, 0).astype(bf16)
     for j in range(send_ref.shape[0]):
         send_ref[j] = message
@@ -166,12 +178,12 @@
 
 
 def last_kernel(row_ref, column_ref, *refs):
-    groups, out_ref = refs[:9], refs[9]
+    groups, out_ref, block_ref, sem = refs[:6], refs[6], refs[7], refs[8]
     carried = before(column_ref, lax.axis_index("z"), None)
     carried = before(row_ref, lax.axis_index("y"), carried)
     back = order_matrix(True).astype(bf16)
-    at = 0
-    for g, name in enumerate(("own", "mid", "end")):
+    at, copies = 0, []
+    for g, name in enumerate(("own", "rest")):
         h_ref, p_ref, edge_ref = groups[3 * g : 3 * g + 3]
         for slot, head in enumerate(heads_of(name)):
             enters = edge_ref[slot, 0] + edge_ref[slot, 1] * carried[at : at + 1]
@@ -179,22 +191,24 @@
                 STEPS, CHUNKS, BLOCK
             ) * enters.reshape(1, CHUNKS, BLOCK)
             rounded = whole.reshape(ROWS, BLOCK).astype(bf16)
+            block_ref[at] = jnp.dot(back, rounded, preferred_element_type=f32).astype(bf16)
             cols = pl.ds(pl.multiple_of(head * BLOCK, BLOCK), BLOCK)
-            out_ref[:, cols] = jnp.dot(back, rounded, preferred_element_type=f32).astype(bf16)
+            copies.append(pltpu.make_async_copy(block_ref.at[at], out_ref.at[:, cols], sem.at[at]))
+            copies[-1].start()
             at += 1
-
-
-def vmem(count):
-    return [pl.BlockSpec(memory_space=pltpu.VMEM)] * count
-
-
-def call(kernel, outs, args, scratch=True, us=2.0):
+    for copy in copies:
+        copy.wait()
+
+
+def call(kernel, outs, args, scratch=None, out_space=pltpu.VMEM, us=2.0):
+    if scratch is None:
+        scratch = [pltpu.VMEM((3, ROWS, BLOCK), f32)]
     return pl.pallas_call(
         kernel,
         out_shape=[jax.ShapeDtypeStruct(s, d) for s, d in outs],
-        in_specs=vmem(len(args)),
-        out_specs=vmem(len(outs)),
-        scratch_shapes=[pltpu.VMEM((3, ROWS, BLOCK), f32)] if scratch else [],
+        in_specs=[pl.BlockSpec(memory_space=pltpu.VMEM)] * len(args),
+        out_specs=[pl.BlockSpec(memory_space=out_space)] * len(outs),
+        scratch_shapes=scratch,
         compiler_params=pltpu.CompilerParams(vmem_limit_bytes=16 * 2**20),
         cost_estimate=pl.CostEstimate(
             flops=int(us * 2e8), bytes_accessed=1 << 20, transcendentals=1 << 18
@@ -216,35 +230,44 @@
         pairs = [(2 * i + c, 2 * ((i + (way, -way)[c]) % 4) + c) for i in range(4) for c in (0, 1)]
         return lax.ppermute(array, dp, pairs)
 
-    def swapped(array):
-        return lax.ppermute(array, "dp_1", [(0, 1), (1, 0)])
-
     own = gate_weight[:, 0]
+    (perm,) = call(order_kernel, [((ROWS, ROWS), bf16)], (), scratch=[], us=50.0)
     first = along(own, 1)
     second = along(own, -1)
-    halo = lax.ppermute(x[ROWS - 8 :], sp, [(i, i + 1) for i in range(columns * lines - 1)])
+    moved, tail = call(
+        move_kernel,
+        [((ROWS, HEADS * BLOCK), bf16), ((8, HEADS * BLOCK), bf16)],
+        (x, perm),
+        scratch=[],
+    )
+    halo = lax.ppermute(tail, sp, [(i, i + 1) for i in range(columns * lines - 1)])
     far = along(first, 1)
-    cv, pcol, ours, *own_out, own_tot = call(
+    cv, ours = call(
+        conv_kernel,
+        [((ROWS, HEADS * BLOCK), bf16), ((3, 2, BLOCK, BLOCK), bf16)],
+        (moved, halo, conv_weight, own, first, second),
+        scratch=[],
+    )
+    theirs = lax.ppermute(ours, "dp_1", [(0, 1), (1, 0)])
+    pcol, *own_out, own_tot = call(
         own_kernel,
-        [
-            ((ROWS, HEADS * BLOCK), bf16),
-            ((ROWS, LANES), f32),
-            ((3, 2, BLOCK, BLOCK), bf16),
-            *head_outs(3),
-            ((2, 3, BLOCK), f32),
-        ],
-        (x, halo, conv_weight, rate, pace, own, first, second),
-    )
-    theirs = swapped(ours)
-    far_theirs = swapped(far)
-    *mid_out, mid_tot = call(mid_kernel, [*head_outs(4), ((2, 4, BLOCK), f32)], (cv, pcol, rate, far, theirs))
+        [((ROWS, LANES), f32), *head_outs(3), ((2, 3, BLOCK), f32)],
+        (cv, rate, pace, own, first, second),
+    )
+    far_pair = lax.all_gather(far, "dp_1")
     message = ((lines, 2 * HEADS, BLOCK), bf16)
-    *end_out, send = call(end_kernel, [*head_outs(1), message], (cv, pcol, rate, far_theirs, own_tot, mid_tot))
+    *rest_out, send = call(
+        rest_kernel, [*head_outs(5), message], (cv, pcol, rate, far_pair, theirs, own_tot)
+    )
     row = lax.all_to_all(send, "y", split_axis=0, concat_axis=0, tiled=True)
-    (send,) = call(row_kernel, [((columns, 2 * HEADS, BLOCK), bf16)], (row,), scratch=False)
+    (send,) = call(row_kernel, [((columns, 2 * HEADS, BLOCK), bf16)], (row,), scratch=[])
     column = lax.all_to_all(send, "z", split_axis=0, concat_axis=0, tiled=True)
     (result,) = call(
-        last_kernel, [((ROWS, HEADS * BLOCK), bf16)], (row, column, *own_out, *mid_out, *end_out), scratch=False
+        last_kernel,
+        [((ROWS, HEADS * BLOCK), bf16)],
+        (row, column, *own_out, *rest_out),
+        scratch=[pltpu.VMEM((HEADS, ROWS, BLOCK), bf16), pltpu.SemaphoreType.DMA((HEADS,))],
+        out_space=pl.ANY,
     )
     return result[None]
 

time: 68 us -> 64.2 us (0.944)
  the two profiles are of different devices: /device:TPU:8 before, /device:TPU:6 now
where the time goes in v3:
time: 64.2 us; the launch traced here: 63.8 us
  blocking collectives  35.6 us (55%)
  starting transfers between devices  18.5 us (29%)
  waiting for transfers between devices  5.5 us (9%)
  Pallas kernels  4.06 us (6%)
    all_to_all x1, blocking collectives, layer(): column = lax.all_to_all(send, 'z', split_axis=0, concat_axis=0, tiled=True)  18.5 us
    ppermute x3, starting transfers between devices, along(): return lax.ppermute(array, dp, pairs)  15.3 us
    all_to_all x1, blocking collectives, layer(): row = lax.all_to_all(send, 'y', split_axis=0, concat_axis=0, tiled=True)  15 us
    pallas_call x7, Pallas kernels, call(): pl.pallas_call(kernel, out_shape=[jax.ShapeDtypeStruct(s, d) for s, d in...  4.06 us
    ppermute x3, waiting for transfers between devices, along(): return lax.ppermute(array, dp, pairs)  3.92 us
    all_gather x1, blocking collectives, layer(): far_pair = lax.all_gather(far, 'dp_1')  2.17 us
    ppermute x1, starting transfers between devices, layer(): theirs = lax.ppermute(ours, 'dp_1', [(0, 1), (1, 0)])  1.92 us
    ppermute x1, waiting for transfers between devices, layer(): lax.ppermute(tail, sp, [(i, i + 1) for i in range(columns * lines - 1)])  1.58 us
  transfers between devices with their start and end apart: 5, of which 4 were waited for; matrix products, arithmetic and copies ran while one was open for 0% of the time, Pallas kernels for 2%

profile of v3, /device:TPU:6, one launch (start us, length us, event | category | flops | bytes accessed | tf_op | source)
XLA Modules:
  0.0 63.8 jit_solution(5076444861628553714)
XLA Ops:
  0.0 0.0 copy-start.1
  0.0 2.9 %collective-permute-start.2 = (bf16[2,256,256]{2,1,0:T(8,128)(2,1)}, bf16[2,256,256]{2,1,0:T(8,128)(2,1)S(1)}, u32[]{:S(2)}, u32[]{:S(2)}) collective-permute-start(bf16[2,256,256]{2,1,0:T(8,128)(2,1)} %bitcast.9), channel_id=1, source_target_pairs={{0,6},{1,3},{2,0},{3,5},{4,2},{5,7},{6,4},{7,1},{8,14},{9,11},{10,... | collective-permute-start | bytes 786440 | tf_op jit(solution)/shard_map/ppermute | solution.py:231
  2.9 6.9 %collective-permute-start.1 = (bf16[2,256,256]{2,1,0:T(8,128)(2,1)}, bf16[2,256,256]{2,1,0:T(8,128)(2,1)S(1)}, u32[]{:S(2)}, u32[]{:S(2)}) collective-permute-start(bf16[2,256,256]{2,1,0:T(8,128)(2,1)} %bitcast.10), channel_id=1, source_target_pairs={{0,2},{1,7},{2,4},{3,1},{4,6},{5,3},{6,0},{7,5},{8,10},{9,15},{10,... | collective-permute-start | bytes 786440 | tf_op jit(solution)/shard_map/ppermute | solution.py:231
  9.8 0.0 copy-done.1
  9.8 0.0 copy-start.2
  9.8 0.0 copy-start.4
  9.9 0.3 shard_map.56
  10.1 1.3 %collective-permute-start = (bf16[8,2048]{1,0:T(8,128)(2,1)S(1)}, bf16[8,2048]{1,0:T(8,128)(2,1)S(1)}, u32[]{:S(2)}, u32[]{:S(2)}) collective-permute-start(bf16[8,2048]{1,0:T(8,128)(2,1)S(1)} %get-tuple-element.19), channel_id=1, source_target_pairs={{0,8},{8,16},{16,24},{24,32},{32,40},{40,48},{48,56},{56,64},{64,7... | collective-permute-start | bytes 98312 | tf_op jit(solution)/shard_map/ppermute | solution.py:243
  11.4 1.6 %collective-permute-done.halo_ref = bf16[8,2048]{1,0:T(8,128)(2,1)S(1)} collective-permute-done((bf16[8,2048]{1,0:T(8,128)(2,1)S(1)}, bf16[8,2048]{1,0:T(8,128)(2,1)S(1)}, u32[]{:S(2)}, u32[]{:S(2)}) %collective-permute-start) | collective-permute-done | bytes 32800 | tf_op jit(solution)/shard_map/ppermute | solution.py:243
  13.0 0.4 collective-permute-done.2.second_ref
  13.4 0.6 collective-permute-done.1.first_ref
  14.0 0.0 copy-done.2
  14.0 0.0 copy-done.4
  14.0 0.0 copy-start
  14.0 0.0 copy-start.3
  14.0 0.4 shard_map.57
  14.4 1.9 %collective-permute-start.4 = (bf16[3,2,256,256]{3,2,1,0:T(8,128)(2,1)S(1)}, bf16[3,2,256,256]{3,2,1,0:T(8,128)(2,1)S(1)}, u32[]{:S(2)}, u32[]{:S(2)}) collective-permute-start(bf16[3,2,256,256]{3,2,1,0:T(8,128)(2,1)S(1)} %get-tuple-element.22), channel_id=1, source_target_pairs={{0,1},{1,0},{2,3},{3,2},{4,5},{5,4},{6,7},{7,6},{8,9},{9,8},{10,11... | collective-permute-start | bytes 2359304 | tf_op jit(solution)/shard_map/ppermute | solution.py:251
  16.3 5.5 %collective-permute-start.3 = (bf16[2,256,256]{2,1,0:T(8,128)(2,1)S(1)}, bf16[2,256,256]{2,1,0:T(8,128)(2,1)S(1)}, u32[]{:S(2)}, u32[]{:S(2)}) collective-permute-start(bf16[2,256,256]{2,1,0:T(8,128)(2,1)S(1)} %collective-permute-done.1.first_ref), channel_id=1, source_target_pairs={{0,2},{1,7},{2,4},{3,1},{4,6},{5,3},{6,0},{7,5},{8,10},{9,15},{10,... | collective-permute-start | bytes 786440 | tf_op jit(solution)/shard_map/ppermute | solution.py:231
  21.8 0.0 copy-done
  21.8 0.0 copy-done.3
  21.8 0.9 %shard_map.58 = (f32[128,128]{1,0:T(8,128)S(1)}, f32[3,128,256]{2,1,0:T(8,128)S(1)}, f32[3,128,256]{2,1,0:T(8,128)S(1)}, f32[3,2,8,256]{3,2,1,0:T(8,128)S(1)}, f32[2,3,256]{2,1,0:T(4,128)S(1)}) custom-call(bf16[128,2048]{1,0:T(8,128)(2,1)S(1)} %get-tuple-element.20.cv_ref, f32[1,2048]{1,0:T(1,128)S(1)} %bitcast.6, f32[1,8192]{1,0:T(1,128)S(1)} %copy-done.3, ...), custom_call_target="tpu_custom_call" | custom-call | flops 400000000 | bytes 1048576 | tf_op jit(solution)/shard_map/pallas_call | solution.py:206
  22.7 3.0 %collective-permute-done.3 = bf16[2,256,256]{2,1,0:T(8,128)(2,1)S(1)} collective-permute-done((bf16[2,256,256]{2,1,0:T(8,128)(2,1)S(1)}, bf16[2,256,256]{2,1,0:T(8,128)(2,1)S(1)}, u32[]{:S(2)}, u32[]{:S(2)}) %collective-permute-start.3) | collective-permute-done | bytes 262176 | tf_op jit(solution)/shard_map/ppermute | solution.py:231
  25.7 2.2 %all-gather = bf16[4,256,256]{2,1,0:T(8,128)(2,1)S(1)} all-gather(bf16[2,256,256]{2,1,0:T(8,128)(2,1)S(1)} %collective-permute-done.3), channel_id=2, replica_groups=mesh['z'=8,'y'=8,'dp_0'=4,'dp_1'=2] {'dp_1'}, dimensions={0}, use_global_device_ids=true | all-gather | bytes 786432 | tf_op jit(solution)/shard_map/all_gather | solution.py:257
  27.9 0.0 collective-permute-done.4.swap_ref
  27.9 1.4 %shard_map.59 = (f32[5,128,256]{2,1,0:T(8,128)S(1)}, f32[5,128,256]{2,1,0:T(8,128)S(1)}, f32[5,2,8,256]{3,2,1,0:T(8,128)S(1)}, bf16[8,16,256]{2,1,0:T(8,128)(2,1)S(1)}) custom-call(bf16[128,2048]{1,0:T(8,128)(2,1)S(1)} %get-tuple-element.20.cv_ref, f32[128,128]{1,0:T(8,128)S(1)} %get-tuple-element.21.pcol_ref, f32[1,2048]{1,0:T(1,128)S(1)} %bitcast.7, ...), custom_call_target="tpu_custom_call" | custom-call | flops 400000000 | bytes 1048576 | tf_op jit(solution)/shard_map/pallas_call | solution.py:206
  29.2 15.0 %all_to_all.10.all_ref.row_ref = bf16[8,16,256]{2,1,0:T(8,128)(2,1)S(1)} all-to-all(bf16[8,16,256]{2,1,0:T(8,128)(2,1)S(1)} %get-tuple-element.24), channel_id=1, replica_groups=mesh['z'=8,'y'=8,'dp_0'=4,'dp_1'=2] {'y'}, dimensions={0} | all-to-all | bytes 131072 | tf_op jit(solution)/shard_map/all_to_all | solution.py:262
  44.2 18.5 %all_to_all.11.column_ref = bf16[8,16,256]{2,1,0:T(8,128)(2,1)S(1)} all-to-all(bf16[8,16,256]{2,1,0:T(8,128)(2,1)S(1)} %shard_map.60), channel_id=1, replica_groups=mesh['z'=8,'y'=8,'dp_0'=4,'dp_1'=2] {'z'}, dimensions={0} | all-to-all | bytes 131072 | tf_op jit(solution)/shard_map/all_to_all | solution.py:264
  62.7 1.1 %shard_map.61 = bf16[128,2048]{1,0:T(8,128)(2,1)} custom-call(bf16[8,16,256]{2,1,0:T(8,128)(2,1)S(1)} %all_to_all.10.all_ref.row_ref, bf16[8,16,256]{2,1,0:T(8,128)(2,1)S(1)} %all_to_all.11.column_ref, f32[3,128,256]{2,1,0:T(8,128)S(1)} %get-tuple-element.25.refs_0_, f32[3,128,256]{2,1,0:T(8,128)S(1)} %get-tuple-element.26.refs_1_, ...), custom_call_target="tpu_custom_call" | custom-call | flops 400000000 | bytes 1048576 | tf_op jit(solution)/shard_map/pallas_call | solution.py:206
  (2 shorter events, 0.1 us)
Async XLA Ops:
  0.0 9.8 %copy-start.1 = (bf16[1,128,2048]{2,1,0:T(8,128)(2,1)S(1)}, bf16[1,128,2048]{2,1,0:T(8,128)(2,1)}, u32[]{:S(2)}) copy-start(bf16[1,128,2048]{2,1,0:T(8,128)(2,1)} %param.5) | copy-start | bytes 1572868
  0.0 13.4 %collective-permute-start.2 = (bf16[2,256,256]{2,1,0:T(8,128)(2,1)}, bf16[2,256,256]{2,1,0:T(8,128)(2,1)S(1)}, u32[]{:S(2)}, u32[]{:S(2)}) collective-permute-start(bf16[2,256,256]{2,1,0:T(8,128)(2,1)} %bitcast.9), channel_id=1, source_target_pairs={{0,6},{1,3},{2,0},{3,5},{4,2},{5,7},{6,4},{7,1},{8,14},{9,11},{10,... | collective-permute-start | bytes 786440 | tf_op jit(solution)/shard_map/ppermute | solution.py:231
  2.9 11.1 %collective-permute-start.1 = (bf16[2,256,256]{2,1,0:T(8,128)(2,1)}, bf16[2,256,256]{2,1,0:T(8,128)(2,1)S(1)}, u32[]{:S(2)}, u32[]{:S(2)}) collective-permute-start(bf16[2,256,256]{2,1,0:T(8,128)(2,1)} %bitcast.10), channel_id=1, source_target_pairs={{0,2},{1,7},{2,4},{3,1},{4,6},{5,3},{6,0},{7,5},{8,10},{9,15},{10,... | collective-permute-start | bytes 786440 | tf_op jit(solution)/shard_map/ppermute | solution.py:231
  9.8 4.1 %copy-start.2 = (bf16[2,1,256,256]{3,2,1,0:T(8,128)(2,1)S(1)}, bf16[2,1,256,256]{3,2,1,0:T(8,128)(2,1)}, u32[]{:S(2)}) copy-start(bf16[2,1,256,256]{3,2,1,0:T(8,128)(2,1)} %param.7) | copy-start | bytes 786436
  9.8 4.1 %copy-start.4 = (bf16[4,2048]{1,0:T(4,128)(2,1)S(1)}, bf16[4,2048]{1,0:T(4,128)(2,1)}, u32[]{:S(2)}) copy-start(bf16[4,2048]{1,0:T(4,128)(2,1)} %cw_ref.1) | copy-start | bytes 49156
  10.1 2.9 %collective-permute-start = (bf16[8,2048]{1,0:T(8,128)(2,1)S(1)}, bf16[8,2048]{1,0:T(8,128)(2,1)S(1)}, u32[]{:S(2)}, u32[]{:S(2)}) collective-permute-start(bf16[8,2048]{1,0:T(8,128)(2,1)S(1)} %get-tuple-element.19), channel_id=1, source_target_pairs={{0,8},{8,16},{16,24},{24,32},{32,40},{40,48},{48,56},{56,64},{64,7... | collective-permute-start | bytes 98312 | tf_op jit(solution)/shard_map/ppermute | solution.py:243
  14.0 7.8 %copy-start = (f32[2048]{0:T(1024)S(1)}, f32[2048]{0:T(1024)}, u32[]{:S(2)}) copy-start(f32[2048]{0:T(1024)} %param.8) | copy-start | bytes 24580
  14.0 7.8 %copy-start.3 = (f32[1,8192]{1,0:T(1,128)S(1)}, f32[1,8192]{1,0:T(1,128)}, u32[]{:S(2)}) copy-start(f32[1,8192]{1,0:T(1,128)} %pace_ref.1) | copy-start | bytes 98308
  14.4 13.5 %collective-permute-start.4 = (bf16[3,2,256,256]{3,2,1,0:T(8,128)(2,1)S(1)}, bf16[3,2,256,256]{3,2,1,0:T(8,128)(2,1)S(1)}, u32[]{:S(2)}, u32[]{:S(2)}) collective-permute-start(bf16[3,2,256,256]{3,2,1,0:T(8,128)(2,1)S(1)} %get-tuple-element.22), channel_id=1, source_target_pairs={{0,1},{1,0},{2,3},{3,2},{4,5},{5,4},{6,7},{7,6},{8,9},{9,8},{10,11... | collective-permute-start | bytes 2359304 | tf_op jit(solution)/shard_map/ppermute | solution.py:251
  16.3 9.4 %collective-permute-start.3 = (bf16[2,256,256]{2,1,0:T(8,128)(2,1)S(1)}, bf16[2,256,256]{2,1,0:T(8,128)(2,1)S(1)}, u32[]{:S(2)}, u32[]{:S(2)}) collective-permute-start(bf16[2,256,256]{2,1,0:T(8,128)(2,1)S(1)} %collective-permute-done.1.first_ref), channel_id=1, source_target_pairs={{0,2},{1,7},{2,4},{3,1},{4,6},{5,3},{6,0},{7,5},{8,10},{9,15},{10,... | collective-permute-start | bytes 786440 | tf_op jit(solution)/shard_map/ppermute | solution.py:231

commit v4 on v3

--- a/solution.py
+++ b/solution.py
@@ -15,6 +15,8 @@
 LANES = 128
 
 
+LOG2E = 1.4426950408889634
+LEAST = 1.1754944e-38
 gate_power = 8.0
 f32, bf16 = jnp.float32, jnp.bfloat16
 
@@ -65,7 +67,7 @@
     pre_ref[0] = jnp.dot(values, w0, preferred_element_type=f32)
     pre_ref[1] = jnp.dot(values, w1, preferred_element_type=f32)
     pre_ref[2] = values.astype(f32)
-    soft = gate_power * softplus_of_minus(rate_ref[:, cols])
+    soft = 2.0 * gate_power * softplus_of_minus(rate_ref[:, cols])
     totals = []
     for lane in range(0, BLOCK, LANES):
         at = slice(lane, lane + LANES)
@@ -75,18 +77,18 @@
             rows = slice(CHUNKS * r, CHUNKS * (r + 1))
             x0 = pre_ref[0, rows, at].astype(bf16).astype(f32)
             x1 = pre_ref[1, rows, at].astype(bf16).astype(f32)
-            recur_gate = 1.0 / (1.0 + jnp.exp(-x0))
-            input_gate = 1.0 / (1.0 + jnp.exp(-x1))
-            loss = pace_ref[rows, :] * recur_gate * soft_here
-            decay = jnp.exp(-loss)
-            v = 2.0 * loss
-            series = v * (1 - v * (1 / 2 - v * (1 / 6 - v * (1 / 24 - v * (1 / 120)))))
-            gone = jnp.where(v < 0.1, series, 1.0 - decay * decay)
-            drive = jnp.sqrt(gone) * input_gate * pre_ref[2, rows, at]
+            recur_gate = 1.0 / (1.0 + jnp.exp2(x0 * -LOG2E))
+            input_gate = 1.0 / (1.0 + jnp.exp2(x1 * -LOG2E))
+            v = pace_ref[rows, :] * recur_gate * soft_here
+            decay = jnp.exp2(v * (-0.5 * LOG2E))
+            series = v * (1 - v * (1 / 2 - v * (1 / 6 - v * (1 / 24))))
+            gone = jnp.where(v < 0.03, series, 1.0 - decay * decay)
+            root = gone * lax.rsqrt(jnp.maximum(gone, LEAST))
+            drive = root * input_gate * pre_ref[2, rows, at]
             if r == 0:
-                state, run, used = drive, decay, loss
+                state, run, used = drive, decay, v
             else:
-                state, run, used = decay * state + drive, decay * run, used + loss
+                state, run, used = decay * state + drive, decay * run, used + v
             h_ref[slot, rows, at] = state
             p_ref[slot, rows, at] = run
         for shift in (1, 2, 4):
@@ -94,7 +96,7 @@
             run = run * sublane_before(run, shift, 1.0)
         edge_ref[slot, 0, :, at] = sublane_before(state, 1, 0.0)
         edge_ref[slot, 1, :, at] = sublane_before(run, 1, 1.0)
-        totals.append((jnp.sum(used, 0, keepdims=True), state[CHUNKS - 1 : CHUNKS]))
+        totals.append((0.5 * jnp.sum(used, 0, keepdims=True), state[CHUNKS - 1 : CHUNKS]))
     return tuple(jnp.concatenate([t[k] for t in totals], 1) for k in (0, 1))
 
 

time: 64.2 us -> 63.8 us (level)
  no operation moved by 1% of the time
where the time goes in v4:
time: 63.8 us; the launch traced here: 63.5 us
  blocking collectives  35.6 us (56%)
  starting transfers between devices  18.5 us (29%)
  waiting for transfers between devices  5.69 us (9%)
  Pallas kernels  3.56 us (6%)
    all_to_all x1, blocking collectives, layer(): column = lax.all_to_all(send, 'z', split_axis=0, concat_axis=0, tiled=True)  18.5 us
    ppermute x3, starting transfers between devices, along(): return lax.ppermute(array, dp, pairs)  15.3 us
    all_to_all x1, blocking collectives, layer(): row = lax.all_to_all(send, 'y', split_axis=0, concat_axis=0, tiled=True)  15 us
    ppermute x3, waiting for transfers between devices, along(): return lax.ppermute(array, dp, pairs)  4.11 us
    pallas_call x7, Pallas kernels, call(): pl.pallas_call(kernel, out_shape=[jax.ShapeDtypeStruct(s, d) for s, d in...  3.56 us
    all_gather x1, blocking collectives, layer(): far_pair = lax.all_gather(far, 'dp_1')  2.17 us
    ppermute x1, starting transfers between devices, layer(): theirs = lax.ppermute(ours, 'dp_1', [(0, 1), (1, 0)])  1.92 us
    ppermute x1, waiting for transfers between devices, layer(): lax.ppermute(tail, sp, [(i, i + 1) for i in range(columns * lines - 1)])  1.58 us
  transfers between devices with their start and end apart: 5, of which 4 were waited for; matrix products, arithmetic and copies ran while one was open for 0% of the time, Pallas kernels for 2%

profile of v4, /device:TPU:6, one launch (start us, length us, event | category | flops | bytes accessed | tf_op | source)
XLA Modules:
  0.0 63.5 jit_solution(17802504469866000836)
XLA Ops:
  0.0 0.0 copy-start.1
  0.0 2.9 %collective-permute-start.2 = (bf16[2,256,256]{2,1,0:T(8,128)(2,1)}, bf16[2,256,256]{2,1,0:T(8,128)(2,1)S(1)}, u32[]{:S(2)}, u32[]{:S(2)}) collective-permute-start(bf16[2,256,256]{2,1,0:T(8,128)(2,1)} %bitcast.9), channel_id=1, source_target_pairs={{0,6},{1,3},{2,0},{3,5},{4,2},{5,7},{6,4},{7,1},{8,14},{9,11},{10,... | collective-permute-start | bytes 786440 | tf_op jit(solution)/shard_map/ppermute | solution.py:233
  2.9 6.9 %collective-permute-start.1 = (bf16[2,256,256]{2,1,0:T(8,128)(2,1)}, bf16[2,256,256]{2,1,0:T(8,128)(2,1)S(1)}, u32[]{:S(2)}, u32[]{:S(2)}) collective-permute-start(bf16[2,256,256]{2,1,0:T(8,128)(2,1)} %bitcast.10), channel_id=1, source_target_pairs={{0,2},{1,7},{2,4},{3,1},{4,6},{5,3},{6,0},{7,5},{8,10},{9,15},{10,... | collective-permute-start | bytes 786440 | tf_op jit(solution)/shard_map/ppermute | solution.py:233
  9.8 0.0 copy-done.1
  9.8 0.0 copy-start.2
  9.8 0.0 copy-start.4
  9.9 0.3 shard_map.56
  10.1 1.3 %collective-permute-start = (bf16[8,2048]{1,0:T(8,128)(2,1)S(1)}, bf16[8,2048]{1,0:T(8,128)(2,1)S(1)}, u32[]{:S(2)}, u32[]{:S(2)}) collective-permute-start(bf16[8,2048]{1,0:T(8,128)(2,1)S(1)} %get-tuple-element.19), channel_id=1, source_target_pairs={{0,8},{8,16},{16,24},{24,32},{32,40},{40,48},{48,56},{56,64},{64,7... | collective-permute-start | bytes 98312 | tf_op jit(solution)/shard_map/ppermute | solution.py:245
  11.4 1.6 %collective-permute-done.halo_ref = bf16[8,2048]{1,0:T(8,128)(2,1)S(1)} collective-permute-done((bf16[8,2048]{1,0:T(8,128)(2,1)S(1)}, bf16[8,2048]{1,0:T(8,128)(2,1)S(1)}, u32[]{:S(2)}, u32[]{:S(2)}) %collective-permute-start) | collective-permute-done | bytes 32800 | tf_op jit(solution)/shard_map/ppermute | solution.py:245
  13.0 0.4 collective-permute-done.2.second_ref
  13.4 0.6 collective-permute-done.1.first_ref
  14.0 0.0 copy-done.2
  14.0 0.0 copy-done.4
  14.0 0.0 copy-start
  14.0 0.0 copy-start.3
  14.0 0.4 shard_map.57
  14.4 1.9 %collective-permute-start.4 = (bf16[3,2,256,256]{3,2,1,0:T(8,128)(2,1)S(1)}, bf16[3,2,256,256]{3,2,1,0:T(8,128)(2,1)S(1)}, u32[]{:S(2)}, u32[]{:S(2)}) collective-permute-start(bf16[3,2,256,256]{3,2,1,0:T(8,128)(2,1)S(1)} %get-tuple-element.22), channel_id=1, source_target_pairs={{0,1},{1,0},{2,3},{3,2},{4,5},{5,4},{6,7},{7,6},{8,9},{9,8},{10,11... | collective-permute-start | bytes 2359304 | tf_op jit(solution)/shard_map/ppermute | solution.py:253
  16.3 5.5 %collective-permute-start.3 = (bf16[2,256,256]{2,1,0:T(8,128)(2,1)S(1)}, bf16[2,256,256]{2,1,0:T(8,128)(2,1)S(1)}, u32[]{:S(2)}, u32[]{:S(2)}) collective-permute-start(bf16[2,256,256]{2,1,0:T(8,128)(2,1)S(1)} %collective-permute-done.1.first_ref), channel_id=1, source_target_pairs={{0,2},{1,7},{2,4},{3,1},{4,6},{5,3},{6,0},{7,5},{8,10},{9,15},{10,... | collective-permute-start | bytes 786440 | tf_op jit(solution)/shard_map/ppermute | solution.py:233
  21.8 0.0 copy-done
  21.8 0.0 copy-done.3
  21.8 0.7 %shard_map.58 = (f32[128,128]{1,0:T(8,128)S(1)}, f32[3,128,256]{2,1,0:T(8,128)S(1)}, f32[3,128,256]{2,1,0:T(8,128)S(1)}, f32[3,2,8,256]{3,2,1,0:T(8,128)S(1)}, f32[2,3,256]{2,1,0:T(4,128)S(1)}) custom-call(bf16[128,2048]{1,0:T(8,128)(2,1)S(1)} %get-tuple-element.20.cv_ref, f32[1,2048]{1,0:T(1,128)S(1)} %bitcast.6, f32[1,8192]{1,0:T(1,128)S(1)} %copy-done.3, ...), custom_call_target="tpu_custom_call" | custom-call | flops 400000000 | bytes 1048576 | tf_op jit(solution)/shard_map/pallas_call | solution.py:208
  22.5 3.2 %collective-permute-done.3 = bf16[2,256,256]{2,1,0:T(8,128)(2,1)S(1)} collective-permute-done((bf16[2,256,256]{2,1,0:T(8,128)(2,1)S(1)}, bf16[2,256,256]{2,1,0:T(8,128)(2,1)S(1)}, u32[]{:S(2)}, u32[]{:S(2)}) %collective-permute-start.3) | collective-permute-done | bytes 262176 | tf_op jit(solution)/shard_map/ppermute | solution.py:233
  25.7 2.2 %all-gather = bf16[4,256,256]{2,1,0:T(8,128)(2,1)S(1)} all-gather(bf16[2,256,256]{2,1,0:T(8,128)(2,1)S(1)} %collective-permute-done.3), channel_id=2, replica_groups=mesh['z'=8,'y'=8,'dp_0'=4,'dp_1'=2] {'dp_1'}, dimensions={0}, use_global_device_ids=true | all-gather | bytes 786432 | tf_op jit(solution)/shard_map/all_gather | solution.py:259
  27.9 0.0 collective-permute-done.4.swap_ref
  27.9 1.0 %shard_map.59 = (f32[5,128,256]{2,1,0:T(8,128)S(1)}, f32[5,128,256]{2,1,0:T(8,128)S(1)}, f32[5,2,8,256]{3,2,1,0:T(8,128)S(1)}, bf16[8,16,256]{2,1,0:T(8,128)(2,1)S(1)}) custom-call(bf16[128,2048]{1,0:T(8,128)(2,1)S(1)} %get-tuple-element.20.cv_ref, f32[128,128]{1,0:T(8,128)S(1)} %get-tuple-element.21.pcol_ref, f32[1,2048]{1,0:T(1,128)S(1)} %bitcast.7, ...), custom_call_target="tpu_custom_call" | custom-call | flops 400000000 | bytes 1048576 | tf_op jit(solution)/shard_map/pallas_call | solution.py:208
  28.9 15.0 %all_to_all.10.all_ref.row_ref = bf16[8,16,256]{2,1,0:T(8,128)(2,1)S(1)} all-to-all(bf16[8,16,256]{2,1,0:T(8,128)(2,1)S(1)} %get-tuple-element.24), channel_id=1, replica_groups=mesh['z'=8,'y'=8,'dp_0'=4,'dp_1'=2] {'y'}, dimensions={0} | all-to-all | bytes 131072 | tf_op jit(solution)/shard_map/all_to_all | solution.py:264
  43.9 18.5 %all_to_all.11.column_ref = bf16[8,16,256]{2,1,0:T(8,128)(2,1)S(1)} all-to-all(bf16[8,16,256]{2,1,0:T(8,128)(2,1)S(1)} %shard_map.60), channel_id=1, replica_groups=mesh['z'=8,'y'=8,'dp_0'=4,'dp_1'=2] {'z'}, dimensions={0} | all-to-all | bytes 131072 | tf_op jit(solution)/shard_map/all_to_all | solution.py:266
  62.4 1.1 %shard_map.61 = bf16[128,2048]{1,0:T(8,128)(2,1)} custom-call(bf16[8,16,256]{2,1,0:T(8,128)(2,1)S(1)} %all_to_all.10.all_ref.row_ref, bf16[8,16,256]{2,1,0:T(8,128)(2,1)S(1)} %all_to_all.11.column_ref, f32[3,128,256]{2,1,0:T(8,128)S(1)} %get-tuple-element.25.refs_0_, f32[3,128,256]{2,1,0:T(8,128)S(1)} %get-tuple-element.26.refs_1_, ...), custom_call_target="tpu_custom_call" | custom-call | flops 400000000 | bytes 1048576 | tf_op jit(solution)/shard_map/pallas_call | solution.py:208
  (2 shorter events, 0.1 us)
Async XLA Ops:
  0.0 9.8 %copy-start.1 = (bf16[1,128,2048]{2,1,0:T(8,128)(2,1)S(1)}, bf16[1,128,2048]{2,1,0:T(8,128)(2,1)}, u32[]{:S(2)}) copy-start(bf16[1,128,2048]{2,1,0:T(8,128)(2,1)} %param.5) | copy-start | bytes 1572868
  0.0 13.4 %collective-permute-start.2 = (bf16[2,256,256]{2,1,0:T(8,128)(2,1)}, bf16[2,256,256]{2,1,0:T(8,128)(2,1)S(1)}, u32[]{:S(2)}, u32[]{:S(2)}) collective-permute-start(bf16[2,256,256]{2,1,0:T(8,128)(2,1)} %bitcast.9), channel_id=1, source_target_pairs={{0,6},{1,3},{2,0},{3,5},{4,2},{5,7},{6,4},{7,1},{8,14},{9,11},{10,... | collective-permute-start | bytes 786440 | tf_op jit(solution)/shard_map/ppermute | solution.py:233
  2.9 11.1 %collective-permute-start.1 = (bf16[2,256,256]{2,1,0:T(8,128)(2,1)}, bf16[2,256,256]{2,1,0:T(8,128)(2,1)S(1)}, u32[]{:S(2)}, u32[]{:S(2)}) collective-permute-start(bf16[2,256,256]{2,1,0:T(8,128)(2,1)} %bitcast.10), channel_id=1, source_target_pairs={{0,2},{1,7},{2,4},{3,1},{4,6},{5,3},{6,0},{7,5},{8,10},{9,15},{10,... | collective-permute-start | bytes 786440 | tf_op jit(solution)/shard_map/ppermute | solution.py:233
  9.8 4.1 %copy-start.2 = (bf16[2,1,256,256]{3,2,1,0:T(8,128)(2,1)S(1)}, bf16[2,1,256,256]{3,2,1,0:T(8,128)(2,1)}, u32[]{:S(2)}) copy-start(bf16[2,1,256,256]{3,2,1,0:T(8,128)(2,1)} %param.7) | copy-start | bytes 786436
  9.8 4.1 %copy-start.4 = (bf16[4,2048]{1,0:T(4,128)(2,1)S(1)}, bf16[4,2048]{1,0:T(4,128)(2,1)}, u32[]{:S(2)}) copy-start(bf16[4,2048]{1,0:T(4,128)(2,1)} %cw_ref.1) | copy-start | bytes 49156
  10.1 2.9 %collective-permute-start = (bf16[8,2048]{1,0:T(8,128)(2,1)S(1)}, bf16[8,2048]{1,0:T(8,128)(2,1)S(1)}, u32[]{:S(2)}, u32[]{:S(2)}) collective-permute-start(bf16[8,2048]{1,0:T(8,128)(2,1)S(1)} %get-tuple-element.19), channel_id=1, source_target_pairs={{0,8},{8,16},{16,24},{24,32},{32,40},{40,48},{48,56},{56,64},{64,7... | collective-permute-start | bytes 98312 | tf_op jit(solution)/shard_map/ppermute | solution.py:245
  14.0 7.8 %copy-start = (f32[2048]{0:T(1024)S(1)}, f32[2048]{0:T(1024)}, u32[]{:S(2)}) copy-start(f32[2048]{0:T(1024)} %param.8) | copy-start | bytes 24580
  14.0 7.8 %copy-start.3 = (f32[1,8192]{1,0:T(1,128)S(1)}, f32[1,8192]{1,0:T(1,128)}, u32[]{:S(2)}) copy-start(f32[1,8192]{1,0:T(1,128)} %pace_ref.1) | copy-start | bytes 98308
  14.4 13.5 %collective-permute-start.4 = (bf16[3,2,256,256]{3,2,1,0:T(8,128)(2,1)S(1)}, bf16[3,2,256,256]{3,2,1,0:T(8,128)(2,1)S(1)}, u32[]{:S(2)}, u32[]{:S(2)}) collective-permute-start(bf16[3,2,256,256]{3,2,1,0:T(8,128)(2,1)S(1)} %get-tuple-element.22), channel_id=1, source_target_pairs={{0,1},{1,0},{2,3},{3,2},{4,5},{5,4},{6,7},{7,6},{8,9},{9,8},{10,11... | collective-permute-start | bytes 2359304 | tf_op jit(solution)/shard_map/ppermute | solution.py:253
  16.3 9.4 %collective-permute-start.3 = (bf16[2,256,256]{2,1,0:T(8,128)(2,1)S(1)}, bf16[2,256,256]{2,1,0:T(8,128)(2,1)S(1)}, u32[]{:S(2)}, u32[]{:S(2)}) collective-permute-start(bf16[2,256,256]{2,1,0:T(8,128)(2,1)S(1)} %collective-permute-done.1.first_ref), channel_id=1, source_target_pairs={{0,2},{1,7},{2,4},{3,1},{4,6},{5,3},{6,0},{7,5},{8,10},{9,15},{10,... | collective-permute-start | bytes 786440 | tf_op jit(solution)/shard_map/ppermute | solution.py:233
